TPU v7x, 512 devices: a 4x2x32 block of a 4x8x32 slice. The times are simulated.
512 devices in a mesh: grp: 2 (over y), fs: 32 (over z), tp: 8 (over x, core).
Axes of the slice: x: 4, y: 2, z: 32, core: 2. Of those that a mesh axis runs over, the one named last changes fastest.
The devices are a block of a 4x8x32 slice.
Arguments:
- stream: bfloat16 [64, 128, 2048], P(('grp', 'fs')), parts along dimension 0, may hold values from -6 to 6
- in_gain: float32 [2048], replicated, may hold values from 0.2 to 5
- value_weight: bfloat16 [2048, 1024], P('fs', 'tp'), may hold values from -0.125 to 0.125
- gate_weight: bfloat16 [2048, 1024], P('fs', 'tp'), may hold values from -0.125 to 0.125
- conv_kernel: bfloat16 [31, 1024], P(None, 'tp'), may hold values from -3.6 to 3.6
- conv_gain: float32 [1024], P('tp'), may hold values from 0.1 to 1.9
- conv_shift: float32 [1024], P('tp'), may hold values from -3 to 3
- out_weight: bfloat16 [1024, 2048], P('tp', 'fs'), may hold values from -0.1875 to 0.1875
- norm_gain: float32 [2048], replicated, may hold values from 0.2 to 5
- up_weight: bfloat16 [2048, 8192], P('fs', 'tp'), may hold values from -0.125 to 0.125
- down_weight: bfloat16 [8192, 2048], P('tp', 'fs'), may hold values from -0.0625 to 0.0625
- out_gain: float32 [2048], P('tp'), may hold values from 0.1 to 1.9
Outputs:
- result: bfloat16 [64, 128, 2048], P(('grp', 'fs'), None, 'tp'), parts along dimension 0
There are 2 independent parts, one for each index of `grp`. A program takes and returns all parts, laid end to end along the dimension named above; an argument that names none is the same for every part. Nothing has to cross between parts.
All inputs are finite; a program needn't handle non-finite values.
Results may differ from a plain program's by a relative error of at most 0.02.
Values may be sent and summed in bfloat16 or wider, within the bound.
No kernel may reach another device: no remote copies, remote signals or barrier semaphores. Data moves between devices by JAX's collectives and lax.ppermute only.
A program may use at most 64 MiB of HBM per device.

v0:
```python
import jax
import jax.numpy as jnp
from jax import lax
from jax.sharding import PartitionSpec as P

KW = 31


norm_epsilon = 1e-05
residual_scale = 2.0**0.25


def in_one_piece(arrays, axis, dim, along):
    widths = [a.shape[along] for a in arrays]
    both = jnp.concatenate(arrays, axis=along)
    out = lax.all_gather(both, axis, axis=dim, tiled=True)
    return tuple(jnp.split(out, [sum(widths[:k]) for k in range(1, len(widths))], axis=along))


def copy_for_each(x, axis):
    length = lax.axis_size(axis)
    return lax.all_to_all(jnp.broadcast_to(x[None], (length, *x.shape)), axis, 0, 0, tiled=True)


def over_copies(x, axis):
    everything = copy_for_each(x, axis)
    return jnp.sum(everything, axis=0)


def gathered_total(x, axis):
    tiles = lax.all_gather(x, axis).astype(jnp.float32)
    return tiles.sum(axis=0)


def in_blocks(x, dim, length):
    dims = x.shape
    tiles = x.reshape(*dims[:dim], length, dims[dim] // length, *dims[dim + 1 :])
    return jnp.moveaxis(tiles, dim, 0)


def summed_on_arrival(x, axis, dim):
    length = lax.axis_size(axis)
    tiles = lax.all_to_all(in_blocks(x, dim, length), axis, 0, 0, tiled=True)
    return jnp.sum(tiles.astype(jnp.float32), axis=0)


def norm_rows(values, gain_vector):
    row_mean = jnp.mean(values, axis=-1, keepdims=True)
    row_var = jnp.mean(jnp.square(values - row_mean), axis=-1, keepdims=True)
    return (values - row_mean) * lax.rsqrt(row_var + norm_epsilon) * gain_vector


def norm_shares(summed, stat_sums, full_width, gain_vector):
    row_mean = stat_sums[0] / full_width
    row_var = stat_sums[1] / full_width - row_mean * row_mean
    return (summed - row_mean[:, None]) * lax.rsqrt(row_var + norm_epsilon)[:, None] * gain_vector


def row_sums(summed):
    return (jnp.sum(summed, axis=1), jnp.sum(summed * summed, axis=1))


def contract(left, turned):
    return lax.dot_general(
        left, turned, (((1,), (1,)), ((), ())), preferred_element_type=jnp.float32
    )


def shards(
    stream,
    in_gain,
    value_weight,
    gate_weight,
    conv_kernel,
    conv_gain,
    conv_shift,
    out_weight,
    norm_gain,
    up_weight,
    down_weight,
    out_gain,
):
    seq_count, seq_length, model_width = stream.shape
    token_count = seq_count * seq_length
    tp_count = lax.axis_size("tp")
    slice_width = model_width // tp_count
    tp_index = lax.axis_index("tp")
    out_turned_shard = out_weight.T
    down_turned_shard = down_weight.T
    value_whole, gate_whole, out_turned, up_whole, down_turned = in_one_piece(
        (value_weight, gate_weight, out_turned_shard, up_weight, down_turned_shard), "fs", 0, 1
    )
    normed = norm_rows(
        stream.reshape(token_count, model_width).astype(jnp.float32), in_gain
    ).astype(jnp.bfloat16)
    channels = value_weight.shape[1]
    values = jnp.dot(normed, value_whole, preferred_element_type=jnp.float32)
    gating = jnp.dot(normed, gate_whole, preferred_element_type=jnp.float32)
    gated = (values * jax.nn.sigmoid(gating)).astype(jnp.bfloat16)
    convolved = lax.conv_general_dilated(
        gated.reshape(seq_count, seq_length, channels),
        conv_kernel[:, None, :],
        window_strides=(1,),
        padding=[(KW - 1, 0)],
        dimension_numbers=("NWC", "WIO", "NWC"),
        feature_group_count=channels,
        preferred_element_type=jnp.float32,
    ).reshape(token_count, channels)
    conv_sums = jax.tree.map(lambda part: over_copies(part, "tp"), row_sums(convolved))
    activated = jax.nn.silu(
        norm_shares(convolved, conv_sums, channels * tp_count, conv_gain) + conv_shift
    ).astype(jnp.bfloat16)
    partial_terms = contract(activated, out_turned)
    mixed = (
        gathered_total(partial_terms.astype(jnp.bfloat16), "tp")
        .astype(jnp.float32)
        .astype(jnp.bfloat16)
    )
    settled_full = norm_rows(
        residual_scale * normed.astype(jnp.float32) + mixed.astype(jnp.float32), norm_gain
    ).astype(jnp.bfloat16)
    settled_own = lax.dynamic_slice_in_dim(settled_full, tp_index * slice_width, slice_width, 1)
    hidden = jnp.square(
        jax.nn.relu(jnp.dot(settled_full, up_whole, preferred_element_type=jnp.float32))
    ).astype(jnp.bfloat16)
    fed_terms = contract(hidden, down_turned)
    fed = summed_on_arrival(fed_terms.astype(jnp.bfloat16), "tp", 1).astype(jnp.bfloat16)
    final_sum = residual_scale * settled_own.astype(jnp.float32) + fed.astype(jnp.float32)
    out_sums = jax.tree.map(lambda part: over_copies(part, "tp"), row_sums(final_sum))
    result = norm_shares(final_sum, out_sums, model_width, out_gain).astype(jnp.bfloat16)
    return result.reshape(seq_count, seq_length, slice_width)


def solution(mesh):
    in_specs = (
        P(("grp", "fs"), None, None),
        P(),
        P("fs", "tp"),
        P("fs", "tp"),
        P(None, "tp"),
        P("tp"),
        P("tp"),
        P("tp", "fs"),
        P(),
        P("fs", "tp"),
        P("tp", "fs"),
        P("tp"),
    )
    out_specs = P(("grp", "fs"), None, "tp")
    return jax.shard_map(shards, mesh=mesh, in_specs=in_specs, out_specs=out_specs, check_vma=False)
```

profile of v0, /device:TPU:33, one launch (start us, length us, event | category | flops | bytes accessed | tf_op | source)
XLA Modules:
  0.0 302.8 jit_solution(11429496831366328836)
XLA Ops:
  6.5 0.0 copy-start
  6.6 0.0 copy-start.1
  6.6 0.0 copy-start.3
  6.6 0.1 all-gather.4.cloned.1.call-start
  6.6 0.8 constant_dynamic-update-slice_fusion.2
  7.4 0.7 constant_dynamic-update-slice_fusion.1
  8.1 0.7 bitcast_dynamic-update-slice_fusion.1
  8.8 0.9 constant_dynamic-update-slice_fusion
  9.8 0.9 bitcast_dynamic-update-slice_fusion
  10.7 0.0 copy-start.2
  10.7 0.7 copy-done.2
  11.4 0.1 all-gather.4.cloned.1.call-update
  11.5 1.2 convert_reduce_fusion
  12.7 1.3 fusion.27
  14.0 159.9 %all-gather.4.cloned.1.call-done = bf16[2048,2432]{1,0:T(8,128)(2,1)} async-done(((bf16[64,2432]{1,0:T(8,128)(2,1)}), bf16[2048,2432]{1,0:T(8,128)(2,1)}) %all-gather.4.cloned.1.call-update) | async-done | bytes 9961488 | tf_op jit(solution)/shard_map/all_gather | solution.py:16
  173.9 1.6 fusion.33
  175.5 1.6 fusion.23
  177.1 0.0 copy-done
  177.1 1.1 fusion.50
  178.2 0.1 multiply_reduce_fusion.2
  178.3 26.3 %all_to_all.29 = f32[8,1,128]{2,1,0:T(1,128)S(1)} all-to-all(f32[8,1,128]{2,1,0:T(1,128)S(1)} %broadcast_in_dim.12), channel_id=1, replica_groups=mesh['grp'=2,'fs'=32,'tp'=8] {'tp'}, dimensions={0} | all-to-all | bytes 8192 | tf_op jit(solution)/shard_map/all_to_all | solution.py:22
  204.6 0.6 broadcast_in_dim.11
  205.2 3.9 %all-to-all-start = ((f32[8,1,128]{2,1,0:T(1,128)}), f32[8,1,128]{2,1,0:T(1,128)S(1)}, u32[]{:S(2)}, u32[]{:S(2)}) async-start(f32[8,1,128]{2,1,0:T(1,128)} %broadcast_in_dim.11), calls=%async_computation | async-start | bytes 8192 | tf_op jit(solution)/shard_map/all_to_all | solution.py:22
  209.2 0.0 all-gather.6.cloned.1.call-start
  209.2 4.6 %all-to-all-done = f32[8,1,128]{2,1,0:T(1,128)S(1)} async-done(((f32[8,1,128]{2,1,0:T(1,128)}), f32[8,1,128]{2,1,0:T(1,128)S(1)}, u32[]{:S(2)}, u32[]{:S(2)}) %all-to-all-start) | async-done | bytes 4128 | tf_op jit(solution)/shard_map/all_to_all | solution.py:22
  213.8 2.2 convolution_convert_fusion
  216.0 0.1 all-gather.6.cloned.1.call-update
  216.1 37.8 %all-gather.6.cloned.1.call-done = bf16[1024,2048]{1,0:T(8,128)(2,1)} async-done(((bf16[128,2048]{1,0:T(8,128)(2,1)}), bf16[1024,2048]{1,0:T(8,128)(2,1)}) %all-gather.6.cloned.1.call-update) | async-done | bytes 4194320 | tf_op jit(solution)/shard_map/all_gather | solution.py:31
  253.9 3.0 reduce_sum.138
  256.9 0.0 copy-done.1
  256.9 0.0 copy-done.3
  256.9 0.0 copy-start.5
  256.9 0.4 fusion.30
  257.3 0.5 multiply_reduce_fusion
  257.8 0.0 copy-done.4
  257.9 0.5 multiply_convert_fusion
  258.4 5.6 %fusion.4 = bf16[128,2048]{1,0:T(8,128)(2,1)S(1)} fusion(bf16[2048,2432]{1,0:T(8,128)(2,1)} %all-gather.4.cloned.1.call-done, bf16[128,2048]{1,0:T(8,128)(2,1)S(1)} %multiply_convert_fusion), kind=kOutput, calls=%fused_computation.4 | convolution fusion | flops 1074397184 | bytes 9437184 | tf_op jit(solution)/shard_map/dot_general | solution.py:64
  264.0 0.8 copy.38
  264.8 3.7 %all-to-all-start.2 = ((bf16[8,128,256]{2,1,0:T(8,128)(2,1)}), bf16[8,128,256]{2,1,0:T(8,128)(2,1)S(1)}, u32[]{:S(2)}, u32[]{:S(2)}) async-start(bf16[8,128,256]{2,1,0:T(8,128)(2,1)} %bitcast.44), calls=%async_computation.2 | async-start | bytes 1048576 | tf_op jit(solution)/shard_map/all_to_all | solution.py:43
  268.5 9.4 %all-to-all-done.2 = bf16[8,128,256]{2,1,0:T(8,128)(2,1)S(1)} async-done(((bf16[8,128,256]{2,1,0:T(8,128)(2,1)}), bf16[8,128,256]{2,1,0:T(8,128)(2,1)S(1)}, u32[]{:S(2)}, u32[]{:S(2)}) %all-to-all-start.2) | async-done | bytes 524320 | tf_op jit(solution)/shard_map/all_to_all | solution.py:43
  277.9 0.1 reduce_sum.141
  278.0 0.1 fusion.36
  278.1 8.0 %all_to_all.30 = f32[8,1,128]{2,1,0:T(1,128)S(1)} all-to-all(f32[8,1,128]{2,1,0:T(1,128)S(1)} %broadcast_in_dim.13), channel_id=1, replica_groups=mesh['grp'=2,'fs'=32,'tp'=8] {'tp'}, dimensions={0} | all-to-all | bytes 8192 | tf_op jit(solution)/shard_map/all_to_all | solution.py:22
  286.1 0.6 broadcast_in_dim.14
  286.7 3.9 %all-to-all-start.4 = ((f32[8,1,128]{2,1,0:T(1,128)}), f32[8,1,128]{2,1,0:T(1,128)S(1)}, u32[]{:S(2)}, u32[]{:S(2)}) async-start(f32[8,1,128]{2,1,0:T(1,128)} %broadcast_in_dim.14), calls=%async_computation.4 | async-start | bytes 8192 | tf_op jit(solution)/shard_map/all_to_all | solution.py:22
  290.7 4.6 %all-to-all-done.4 = f32[8,1,128]{2,1,0:T(1,128)S(1)} async-done(((f32[8,1,128]{2,1,0:T(1,128)}), f32[8,1,128]{2,1,0:T(1,128)S(1)}, u32[]{:S(2)}, u32[]{:S(2)}) %all-to-all-start.4) | async-done | bytes 4128 | tf_op jit(solution)/shard_map/all_to_all | solution.py:22
  295.3 0.0 copy-done.5
  295.3 0.7 fusion.37
  (13 shorter events, 0.1 us)
Async XLA Ops:
  6.5 170.6 %copy-start = (bf16[31,128]{1,0:T(8,128)(2,1)S(1)}, bf16[31,128]{1,0:T(8,128)(2,1)}, u32[]{:S(2)}) copy-start(bf16[31,128]{1,0:T(8,128)(2,1)} %param.16) | copy-start | bytes 23812
  6.6 250.3 %copy-start.1 = (bf16[1,128,2048]{2,1,0:T(8,128)(2,1)S(1)}, bf16[1,128,2048]{2,1,0:T(8,128)(2,1)}, u32[]{:S(2)}) copy-start(bf16[1,128,2048]{2,1,0:T(8,128)(2,1)} %param.12) | copy-start | bytes 1572868
  6.6 250.3 %copy-start.3 = (f32[2048]{0:T(1024)S(1)}, f32[2048]{0:T(1024)}, u32[]{:S(2)}) copy-start(f32[2048]{0:T(1024)} %param.13) | copy-start | bytes 24580
  6.6 251.3 %copy-start.4 = (f32[2048]{0:T(1024)S(1)}, f32[2048]{0:T(1024)}, u32[]{:S(2)}) copy-start(f32[2048]{0:T(1024)} %param.20) | copy-start | bytes 24580
  6.6 167.4 %all-gather.4.cloned.1.call-start = ((), (), s32[]{:S(2)}) async-start(), calls=%async_computation.5 | async-start | bytes 10272768 | tf_op jit(solution)/shard_map/all_gather | solution.py:16
  10.7 0.7 copy-start.2
  205.2 8.5 %all-to-all-start = ((f32[8,1,128]{2,1,0:T(1,128)}), f32[8,1,128]{2,1,0:T(1,128)S(1)}, u32[]{:S(2)}, u32[]{:S(2)}) async-start(f32[8,1,128]{2,1,0:T(1,128)} %broadcast_in_dim.11), calls=%async_computation | async-start | bytes 8192 | tf_op jit(solution)/shard_map/all_to_all | solution.py:22
  209.2 44.7 %all-gather.6.cloned.1.call-start = ((), (), s32[]{:S(2)}) async-start(), calls=%async_computation.6 | async-start | bytes 4718592 | tf_op jit(solution)/shard_map/all_gather | solution.py:31
  256.9 38.4 %copy-start.5 = (f32[256]{0:T(256)S(1)}, f32[256]{0:T(256)}, u32[]{:S(2)}) copy-start(f32[256]{0:T(256)} %param.23) | copy-start | bytes 3076
  264.8 13.1 %all-to-all-start.2 = ((bf16[8,128,256]{2,1,0:T(8,128)(2,1)}), bf16[8,128,256]{2,1,0:T(8,128)(2,1)S(1)}, u32[]{:S(2)}, u32[]{:S(2)}) async-start(bf16[8,128,256]{2,1,0:T(8,128)(2,1)} %bitcast.44), calls=%async_computation.2 | async-start | bytes 1048576 | tf_op jit(solution)/shard_map/all_to_all | solution.py:43
  286.7 8.5 %all-to-all-start.4 = ((f32[8,1,128]{2,1,0:T(1,128)}), f32[8,1,128]{2,1,0:T(1,128)S(1)}, u32[]{:S(2)}, u32[]{:S(2)}) async-start(f32[8,1,128]{2,1,0:T(1,128)} %broadcast_in_dim.14), calls=%async_computation.4 | async-start | bytes 8192 | tf_op jit(solution)/shard_map/all_to_all | solution.py:22
Sparse Core Ops, SparseCore 0:
  11.6 162.2 all-gather.3
  216.2 37.6 all-gather.5
where the time goes:
time: 304 us; the launch traced here: 303 us
  waiting for transfers between devices  216 us (71%)
  blocking collectives  34.3 us (11%)
  between operations  13.6 us (4%)
  matrix products  12.1 us (4%)
  starting transfers between devices  11.6 us (4%)
  other arithmetic  8.11 us (3%)
  local copies, waits for them, and re-layouts  6.82 us (2%)
    all_gather x1, waiting for transfers between devices, in_one_piece(): out = lax.all_gather(both, axis, axis=dim, tiled=True)  160 us
    all_gather x1, waiting for transfers between devices, gathered_total(): tiles = lax.all_gather(x, axis).astype(jnp.float32)  37.8 us
    all_to_all x2, blocking collectives, copy_for_each(): lax.all_to_all(jnp.broadcast_to(x[None], (length, *x.shape)), axis, 0, 0,...  34.3 us
    all_to_all x1, waiting for transfers between devices, summed_on_arrival(): tiles = lax.all_to_all(in_blocks(x, dim, length), axis, 0, 0, tiled=True)  9.44 us
    all_to_all x2, waiting for transfers between devices, copy_for_each(): lax.all_to_all(jnp.broadcast_to(x[None], (length, *x.shape)), axis, 0, 0,...  9.13 us
    all_to_all x2, starting transfers between devices, copy_for_each(): lax.all_to_all(jnp.broadcast_to(x[None], (length, *x.shape)), axis, 0, 0,...  7.84 us
    dot_general x2, matrix products, contract(): lax.dot_general(left, turned, (((1,), (1,)), ((), ())), preferred_element...  7.79 us
  transfers between devices with their start and end apart: 5, of which 5 were waited for; matrix products, arithmetic and copies ran while one was open for 1% of the time, Pallas kernels for 0%

commit v1 on v0

v1 whole, which is shorter than its diff:
```python
import jax
import jax.numpy as jnp
from jax import lax
from jax.sharding import PartitionSpec as P

KW = 31

norm_epsilon = 1e-05
residual_scale = 2.0**0.25


def gather_fs(x):
    groups = lax.axis_size("grp")
    rows = x.shape[0] // groups
    own = lax.dynamic_slice_in_dim(x, lax.axis_index("grp") * rows, rows, 0)
    return lax.all_gather(own, ("fs", "grp"), axis=0, tiled=True)


def norm_rows(values, gain_vector):
    row_mean = jnp.mean(values, axis=-1, keepdims=True)
    row_var = jnp.mean(jnp.square(values - row_mean), axis=-1, keepdims=True)
    return (values - row_mean) * lax.rsqrt(row_var + norm_epsilon) * gain_vector


def contract(left, turned):
    return lax.dot_general(
        left, turned, (((1,), (1,)), ((), ())), preferred_element_type=jnp.float32
    )


def swap_blocks(x):
    return lax.all_to_all(x, "tp", 0, 0, tiled=True)


def summed_tokens(terms):
    tp_count = lax.axis_size("tp")
    tokens, width = terms.shape
    tiles = swap_blocks(terms.astype(jnp.bfloat16).reshape(tp_count, tokens // tp_count, width))
    return jnp.sum(tiles.astype(jnp.float32), axis=0).astype(jnp.bfloat16)


def shards(
    stream,
    in_gain,
    value_weight,
    gate_weight,
    conv_kernel,
    conv_gain,
    conv_shift,
    out_weight,
    norm_gain,
    up_weight,
    down_weight,
    out_gain,
):
    seq_count, seq_length, model_width = stream.shape
    token_count = seq_count * seq_length
    tp_count = lax.axis_size("tp")
    slice_width = model_width // tp_count
    own_tokens = token_count // tp_count
    tp_index = lax.axis_index("tp")
    channels = value_weight.shape[1]

    first = gather_fs(jnp.concatenate([value_weight, gate_weight, out_weight.T], axis=1))
    up_weight, first = lax.optimization_barrier((up_weight, first))
    up_whole = gather_fs(up_weight)
    down_weight, up_whole = lax.optimization_barrier((down_weight, up_whole))
    down_turned = gather_fs(down_weight.T)
    value_gate, out_turned = first[:, : 2 * channels], first[:, 2 * channels :]

    normed = norm_rows(
        stream.reshape(token_count, model_width).astype(jnp.float32), in_gain
    ).astype(jnp.bfloat16)
    both = jnp.dot(normed, value_gate, preferred_element_type=jnp.float32)
    gated = (both[:, :channels] * jax.nn.sigmoid(both[:, channels:])).astype(jnp.bfloat16)
    convolved = lax.conv_general_dilated(
        gated.reshape(seq_count, seq_length, channels),
        conv_kernel[:, None, :],
        window_strides=(1,),
        padding=[(KW - 1, 0)],
        dimension_numbers=("NWC", "WIO", "NWC"),
        feature_group_count=channels,
        preferred_element_type=jnp.float32,
    ).reshape(token_count, channels)
    sums = jnp.stack([jnp.sum(convolved, axis=1), jnp.sum(convolved * convolved, axis=1)])
    sums = jnp.sum(swap_blocks(jnp.broadcast_to(sums[None], (tp_count, *sums.shape))), axis=0)
    row_mean = sums[0] / (channels * tp_count)
    row_var = sums[1] / (channels * tp_count) - row_mean * row_mean
    activated = jax.nn.silu(
        (convolved - row_mean[:, None]) * lax.rsqrt(row_var + norm_epsilon)[:, None] * conv_gain
        + conv_shift
    ).astype(jnp.bfloat16)

    mixed = summed_tokens(contract(activated, out_turned))
    normed_own = lax.dynamic_slice_in_dim(normed, tp_index * own_tokens, own_tokens, 0)
    settled_own = norm_rows(
        residual_scale * normed_own.astype(jnp.float32) + mixed.astype(jnp.float32), norm_gain
    ).astype(jnp.bfloat16)
    settled = lax.all_gather(settled_own, "tp", axis=0, tiled=True)
    whole_gain = lax.all_gather(out_gain, "tp", axis=0, tiled=True)

    hidden = jnp.square(
        jax.nn.relu(jnp.dot(settled, up_whole, preferred_element_type=jnp.float32))
    ).astype(jnp.bfloat16)
    fed = summed_tokens(contract(hidden, down_turned))
    result_own = norm_rows(
        residual_scale * settled_own.astype(jnp.float32) + fed.astype(jnp.float32), whole_gain
    ).astype(jnp.bfloat16)
    pieces = jnp.moveaxis(result_own.reshape(own_tokens, tp_count, slice_width), 1, 0)
    result = swap_blocks(pieces)
    return result.reshape(seq_count, seq_length, slice_width)


def solution(mesh):
    in_specs = (
        P(("grp", "fs"), None, None),
        P(),
        P("fs", "tp"),
        P("fs", "tp"),
        P(None, "tp"),
        P("tp"),
        P("tp"),
        P("tp", "fs"),
        P(),
        P("fs", "tp"),
        P("tp", "fs"),
        P("tp"),
    )
    out_specs = P(("grp", "fs"), None, "tp")
    return jax.shard_map(shards, mesh=mesh, in_specs=in_specs, out_specs=out_specs, check_vma=False)
```

time: 304 us -> 905 us (2.98)
  waiting for transfers between devices: 216 us -> 778 us
  blocking collectives: 34.3 us -> 63.5 us
  starting transfers between devices: 11.6 us -> 29.2 us
    all_gather x2 -> x3, waiting for transfers between devices: 198 us -> 768 us  [gather_fs(): return lax.all_gather(own, ('fs', 'grp'), axis=0, tiled=True)]
    all_gather x0 -> x2, blocking collectives: none -> 27.1 us  [the longest x1 14 us: shards(): settled = lax.all_gather(settled_own, 'tp', axis=0, tiled=True)]
    all_to_all x3 -> x2, starting transfers between devices: 11.5 us -> 29 us  [swap_blocks(): return lax.all_to_all(x, 'tp', 0, 0, tiled=True)]
    all_to_all x3 -> x2, waiting for transfers between devices: 18.6 us -> 9.44 us  [swap_blocks(): return lax.all_to_all(x, 'tp', 0, 0, tiled=True)]
  transfers between devices with their start and end apart: 5 -> 5, of which waited for: 5 -> 4; matrix products, arithmetic and copies ran while one was open for 1% -> 1% of each run, Pallas kernels for 0% -> 0%
where the time goes in v1:
time: 905 us; the launch traced here: 904 us
  waiting for transfers between devices  778 us (86%)
  blocking collectives  63.5 us (7%)
  starting transfers between devices  29.2 us (3%)
  between operations  13.3 us (1%)
  matrix products  11.2 us (1%)
    all_gather x3, waiting for transfers between devices, gather_fs(): return lax.all_gather(own, ('fs', 'grp'), axis=0, tiled=True)  768 us
    all_to_all x2, blocking collectives, swap_blocks(): return lax.all_to_all(x, 'tp', 0, 0, tiled=True)  36.4 us
    all_to_all x2, starting transfers between devices, swap_blocks(): return lax.all_to_all(x, 'tp', 0, 0, tiled=True)  29 us
  transfers between devices with their start and end apart: 5, of which 4 were waited for; matrix products, arithmetic and copies ran while one was open for 1% of the time, Pallas kernels for 0%

profile of v1, /device:TPU:33, one launch (start us, length us, event | category | flops | bytes accessed | tf_op | source)
XLA Modules:
  0.0 904.0 jit_solution(4344918902688362367)
XLA Ops:
  6.5 0.0 copy-start
  6.6 0.0 copy-start.5
  6.6 0.0 copy-start.4
  6.6 0.0 copy-start.3
  6.6 0.1 all-gather.5.cloned.1.call-start
  6.6 1.4 fusion.28
  8.0 0.1 all-gather.5.cloned.1.call-update
  8.1 0.1 all-gather.7.cloned.1.call-start
  8.1 277.9 %all-gather.5.cloned.1.call-done = bf16[2048,384]{1,0:T(8,128)(2,1)} async-done(((bf16[32,384]{1,0:T(8,128)(2,1)}), bf16[2048,384]{1,0:T(8,128)(2,1)}) %all-gather.5.cloned.1.call-update) | async-done | bytes 1572880 | tf_op jit(solution)/shard_map/all_gather | solution.py:16
  286.0 0.0 copy-done
  286.0 0.6 constant_dynamic-slice_fusion
  286.7 0.1 all-gather.7.cloned.1.call-update
  286.7 0.1 all-gather.9.cloned.1.call-start
  286.8 278.4 %all-gather.7.cloned.1.call-done = bf16[2048,1024]{1,0:T(8,128)(2,1)} async-done(((bf16[32,1024]{1,0:T(8,128)(2,1)}), bf16[2048,1024]{1,0:T(8,128)(2,1)}) %all-gather.7.cloned.1.call-update) | async-done | bytes 4194320 | tf_op jit(solution)/shard_map/all_gather | solution.py:16
  565.2 1.5 dynamic-slice_bitcast_fusion
  566.7 0.1 all-gather.9.cloned.1.call-update
  566.7 0.0 copy-start.1
  566.7 1.2 convert_reduce_fusion
  567.9 1.3 fusion.5
  569.3 1.4 fusion.7
  570.7 1.5 fusion.8
  572.3 0.0 copy-done.5
  572.3 1.1 fusion.34
  573.4 0.1 multiply_reduce_fusion.2
  573.5 28.9 %all_to_all.20 = f32[8,2,128]{2,1,0:T(2,128)S(1)} all-to-all(f32[8,2,128]{2,1,0:T(2,128)S(1)} %broadcast_in_dim.5), channel_id=1, replica_groups=mesh['grp'=2,'fs'=32,'tp'=8] {'tp'}, dimensions={0} | all-to-all | bytes 16384 | tf_op jit(solution)/shard_map/all_to_all | solution.py:32
  602.5 0.0 copy-done.4
  602.5 0.0 copy-done.3
  602.5 2.2 convolution_convert_fusion.1
  604.7 4.1 all-to-all-start.1
  608.8 9.4 %all-to-all-done.1 = bf16[8,16,2048]{2,1,0:T(8,128)(2,1)S(1)} async-done(((bf16[8,16,2048]{2,1,0:T(8,128)(2,1)}), bf16[8,16,2048]{2,1,0:T(8,128)(2,1)S(1)}, u32[]{:S(2)}, u32[]{:S(2)}) %all-to-all-start.1) | async-done | bytes 524320 | tf_op jit(solution)/shard_map/all_to_all | solution.py:32
  618.2 0.1 reduce_sum.110
  618.3 0.1 fusion.12
  618.5 0.2 multiply_reduce_fusion.1
  618.7 0.0 copy-done.1
  618.7 0.1 multiply_convert_fusion.1
  618.8 14.0 %all_gather.16 = bf16[128,2048]{1,0:T(8,128)(2,1)S(1)} all-gather(bf16[16,2048]{1,0:T(8,128)(2,1)S(1)} %multiply_convert_fusion.1), channel_id=1, replica_groups=mesh['grp'=2,'fs'=32,'tp'=8] {'tp'}, dimensions={0}, use_global_device_ids=true | all-gather | bytes 589824 | tf_op jit(solution)/shard_map/all_gather | solution.py:99
  632.8 211.7 %all-gather.9.cloned.1.call-done = bf16[2048,1024]{1,0:T(8,128)(2,1)} async-done(((bf16[32,1024]{1,0:T(8,128)(2,1)}), bf16[2048,1024]{1,0:T(8,128)(2,1)}) %all-gather.9.cloned.1.call-update) | async-done | bytes 4194320 | tf_op jit(solution)/shard_map/all_gather | solution.py:16
  844.5 6.4 convolution_convert_fusion
  850.8 24.9 %all-to-all-start.2 = ((bf16[8,16,2048]{2,1,0:T(8,128)(2,1)}), bf16[8,16,2048]{2,1,0:T(8,128)(2,1)S(1)}, u32[]{:S(2)}, u32[]{:S(2)}) async-start(bf16[8,16,2048]{2,1,0:T(8,128)(2,1)} %bitcast.11), calls=%async_computation.2 | async-start | bytes 1048576 | tf_op jit(solution)/shard_map/all_to_all | solution.py:32
  875.7 0.0 copy-done.2
  875.7 13.1 %all-gather = f32[8,1,256]{2,1,0:T(1,128)S(1)} all-gather(f32[1,1,256]{2,1,0:T(1,128)S(1)} %bitcast.57), channel_id=1, replica_groups=mesh['grp'=2,'fs'=32,'tp'=8] {'tp'}, dimensions={0}, use_global_device_ids=true | all-gather | bytes 9216 | tf_op jit(solution)/shard_map/all_gather | solution.py:100
  888.8 0.0 all-to-all-done.2
  888.8 0.1 reduce_sum.113
  888.9 0.1 fusion.13
  889.1 0.2 multiply_reduce_fusion
  889.3 0.1 multiply_convert_fusion
  889.4 7.4 all_to_all.21
  896.8 0.6 copy.41
  (14 shorter events, 0.1 us)
Async XLA Ops:
  6.5 279.5 %copy-start = (bf16[64,1024]{1,0:T(8,128)(2,1)S(1)}, bf16[64,1024]{1,0:T(8,128)(2,1)}, u32[]{:S(2)}) copy-start(bf16[64,1024]{1,0:T(8,128)(2,1)} %param.21) | copy-start | bytes 393220
  6.6 565.7 %copy-start.5 = (bf16[31,128]{1,0:T(8,128)(2,1)S(1)}, bf16[31,128]{1,0:T(8,128)(2,1)}, u32[]{:S(2)}) copy-start(bf16[31,128]{1,0:T(8,128)(2,1)} %param.16) | copy-start | bytes 23812
  6.6 595.9 %copy-start.4 = (f32[128]{0:T(128)S(1)}, f32[128]{0:T(128)}, u32[]{:S(2)}) copy-start(f32[128]{0:T(128)} %param.17) | copy-start | bytes 1540
  6.6 595.9 %copy-start.3 = (f32[128]{0:T(128)S(1)}, f32[128]{0:T(128)}, u32[]{:S(2)}) copy-start(f32[128]{0:T(128)} %param.18) | copy-start | bytes 1540
  6.6 279.5 %all-gather.5.cloned.1.call-start = ((), (), s32[]{:S(2)}) async-start(), calls=%async_computation.4 | async-start | bytes 1597440 | tf_op jit(solution)/shard_map/all_gather | solution.py:16
  8.1 557.1 %all-gather.7.cloned.1.call-start = ((), (), s32[]{:S(2)}) async-start(), calls=%async_computation.5 | async-start | bytes 4259840 | tf_op jit(solution)/shard_map/all_gather | solution.py:16
  286.7 557.7 %all-gather.9.cloned.1.call-start = ((), (), s32[]{:S(2)}) async-start(), calls=%async_computation.6 | async-start | bytes 4259840 | tf_op jit(solution)/shard_map/all_gather | solution.py:16
  566.7 52.0 %copy-start.1 = (f32[2048]{0:T(1024)S(1)}, f32[2048]{0:T(1024)}, u32[]{:S(2)}) copy-start(f32[2048]{0:T(1024)} %param.20) | copy-start | bytes 24580
  604.7 13.5 %all-to-all-start.1 = ((bf16[8,16,2048]{2,1,0:T(8,128)(2,1)}), bf16[8,16,2048]{2,1,0:T(8,128)(2,1)S(1)}, u32[]{:S(2)}, u32[]{:S(2)}) async-start(bf16[8,16,2048]{2,1,0:T(8,128)(2,1)} %bitcast.9), calls=%async_computation.1 | async-start | bytes 1048576 | tf_op jit(solution)/shard_map/all_to_all | solution.py:32
  632.8 243.0 %copy-start.2 = (f32[256]{0:T(256)S(1)}, f32[256]{0:T(256)}, u32[]{:S(2)}) copy-start(f32[256]{0:T(256)} %param.23) | copy-start | bytes 3076
  850.8 38.0 %all-to-all-start.2 = ((bf16[8,16,2048]{2,1,0:T(8,128)(2,1)}), bf16[8,16,2048]{2,1,0:T(8,128)(2,1)S(1)}, u32[]{:S(2)}, u32[]{:S(2)}) async-start(bf16[8,16,2048]{2,1,0:T(8,128)(2,1)} %bitcast.11), calls=%async_computation.2 | async-start | bytes 1048576 | tf_op jit(solution)/shard_map/all_to_all | solution.py:32
Sparse Core Ops, SparseCore 0:
  10.5 275.4 all-gather.4
  289.2 275.9 all-gather.6
  568.3 276.0 all-gather.8

commit v2 on v1

--- a/solution.py
+++ b/solution.py
@@ -10,10 +10,17 @@
 
 
 def gather_fs(x):
-    groups = lax.axis_size("grp")
-    rows = x.shape[0] // groups
-    own = lax.dynamic_slice_in_dim(x, lax.axis_index("grp") * rows, rows, 0)
-    return lax.all_gather(own, ("fs", "grp"), axis=0, tiled=True)
+    return lax.all_gather(x, "fs", axis=0, tiled=True)
+
+
+def gather_in_pairs(even_part, odd_part):
+    group_count = lax.axis_size("grp")
+    if group_count % 2:
+        return gather_fs(even_part), gather_fs(odd_part)
+    is_even = lax.axis_index("grp") % 2 == 0
+    mine = gather_fs(jnp.where(is_even, even_part, odd_part))
+    theirs = lax.ppermute(mine, "grp", [(g, g ^ 1) for g in range(group_count)])
+    return jnp.where(is_even, mine, theirs), jnp.where(is_even, theirs, mine)
 
 
 def norm_rows(values, gain_vector):
@@ -61,18 +68,29 @@
     tp_index = lax.axis_index("tp")
     channels = value_weight.shape[1]
 
-    first = gather_fs(jnp.concatenate([value_weight, gate_weight, out_weight.T], axis=1))
-    up_weight, first = lax.optimization_barrier((up_weight, first))
-    up_whole = gather_fs(up_weight)
-    down_weight, up_whole = lax.optimization_barrier((down_weight, up_whole))
-    down_turned = gather_fs(down_weight.T)
-    value_gate, out_turned = first[:, : 2 * channels], first[:, 2 * channels :]
+    feed = gather_fs(jnp.concatenate([up_weight, down_weight.T], axis=1))
+    hidden_count = up_weight.shape[1]
+    up_whole, down_turned = feed[:, :hidden_count], feed[:, hidden_count:]
+
+    rows = value_weight.shape[0]
+    half = rows // 2
+    out_shard = out_weight.T
+    even_whole, odd_whole = gather_in_pairs(
+        jnp.concatenate([value_weight, out_shard[:half]], axis=0),
+        jnp.concatenate([gate_weight, out_shard[half:]], axis=0),
+    )
+    even_whole = even_whole.reshape(-1, rows + half, channels)
+    odd_whole = odd_whole.reshape(-1, rows + half, channels)
+    value_whole = even_whole[:, :rows].reshape(-1, channels)
+    gate_whole = odd_whole[:, :rows].reshape(-1, channels)
+    out_turned = jnp.concatenate([even_whole[:, rows:], odd_whole[:, rows:]], axis=1).reshape(-1, channels)
 
     normed = norm_rows(
         stream.reshape(token_count, model_width).astype(jnp.float32), in_gain
     ).astype(jnp.bfloat16)
-    both = jnp.dot(normed, value_gate, preferred_element_type=jnp.float32)
-    gated = (both[:, :channels] * jax.nn.sigmoid(both[:, channels:])).astype(jnp.bfloat16)
+    values = jnp.dot(normed, value_whole, preferred_element_type=jnp.float32)
+    gating = jnp.dot(normed, gate_whole, preferred_element_type=jnp.float32)
+    gated = (values * jax.nn.sigmoid(gating)).astype(jnp.bfloat16)
     convolved = lax.conv_general_dilated(
         gated.reshape(seq_count, seq_length, channels),
         conv_kernel[:, None, :],
@@ -82,8 +100,12 @@
         feature_group_count=channels,
         preferred_element_type=jnp.float32,
     ).reshape(token_count, channels)
-    sums = jnp.stack([jnp.sum(convolved, axis=1), jnp.sum(convolved * convolved, axis=1)])
-    sums = jnp.sum(swap_blocks(jnp.broadcast_to(sums[None], (tp_count, *sums.shape))), axis=0)
+    told = jnp.concatenate(
+        [jnp.sum(convolved, axis=1), jnp.sum(convolved * convolved, axis=1), out_gain]
+    )
+    heard = swap_blocks(jnp.broadcast_to(told[None], (tp_count, *told.shape)))
+    sums = jnp.sum(heard[:, : 2 * token_count], axis=0).reshape(2, token_count)
+    whole_gain = heard[:, 2 * token_count :].reshape(model_width)
     row_mean = sums[0] / (channels * tp_count)
     row_var = sums[1] / (channels * tp_count) - row_mean * row_mean
     activated = jax.nn.silu(
@@ -97,7 +119,6 @@
         residual_scale * normed_own.astype(jnp.float32) + mixed.astype(jnp.float32), norm_gain
     ).astype(jnp.bfloat16)
     settled = lax.all_gather(settled_own, "tp", axis=0, tiled=True)
-    whole_gain = lax.all_gather(out_gain, "tp", axis=0, tiled=True)
 
     hidden = jnp.square(
         jax.nn.relu(jnp.dot(settled, up_whole, preferred_element_type=jnp.float32))

time: 905 us -> 225 us (0.25)
  waiting for transfers between devices: 778 us -> 31.7 us
  blocking collectives: 63.5 us -> 114 us
  starting transfers between devices: 29.2 us -> 47.3 us
    all_gather x3 -> x1, waiting for transfers between devices: 768 us -> 1.18 us  [gather_fs(): return lax.all_gather(x, 'fs', axis=0, tiled=True)]
    all_gather x1, blocking collectives: 13.1 us -> 91.9 us  [gather_fs(): return lax.all_gather(x, 'fs', axis=0, tiled=True)]
    all_to_all x2 -> x1, blocking collectives: 36.4 us -> 8.25 us  [swap_blocks(): return lax.all_to_all(x, 'tp', 0, 0, tiled=True)]
    all_to_all x2 -> x3, waiting for transfers between devices: 9.44 us -> 23.3 us  [swap_blocks(): return lax.all_to_all(x, 'tp', 0, 0, tiled=True)]
    all_to_all x2 -> x3, starting transfers between devices: 29 us -> 41.6 us  [swap_blocks(): return lax.all_to_all(x, 'tp', 0, 0, tiled=True)]
  transfers between devices with their start and end apart: 5 -> 5, of which waited for: 4 -> 5; matrix products, arithmetic and copies ran while one was open for 1% -> 4% of each run, Pallas kernels for 0% -> 0%
where the time goes in v2:
time: 225 us
  blocking collectives  114 us (51%)
  starting transfers between devices  47.3 us (21%)
  waiting for transfers between devices  31.7 us (14%)
  between operations  13.6 us (6%)
  matrix products  9.45 us (4%)
  other arithmetic  6.39 us (3%)
    all_gather x1, blocking collectives, gather_fs(): return lax.all_gather(x, 'fs', axis=0, tiled=True)  91.9 us
    all_to_all x3, starting transfers between devices, swap_blocks(): return lax.all_to_all(x, 'tp', 0, 0, tiled=True)  41.6 us
    all_to_all x3, waiting for transfers between devices, swap_blocks(): return lax.all_to_all(x, 'tp', 0, 0, tiled=True)  23.3 us
    all_gather x1, blocking collectives, shards(): settled = lax.all_gather(settled_own, 'tp', axis=0, tiled=True)  14 us
    all_to_all x1, blocking collectives, swap_blocks(): return lax.all_to_all(x, 'tp', 0, 0, tiled=True)  8.25 us
    dot_general x2, matrix products, contract(): lax.dot_general(left, turned, (((1,), (1,)), ((), ())), preferred_element...  7.61 us
    ppermute x1, waiting for transfers between devices, gather_in_pairs(): theirs = lax.ppermute(mine, 'grp', [(g, g ^ 1) for g in range(group_count)])  7.2 us
    ppermute x1, starting transfers between devices, gather_in_pairs(): theirs = lax.ppermute(mine, 'grp', [(g, g ^ 1) for g in range(group_count)])  5.63 us
  transfers between devices with their start and end apart: 5, of which 5 were waited for; matrix products, arithmetic and copies ran while one was open for 4% of the time, Pallas kernels for 0%

profile of v2, /device:TPU:33, one launch (start us, length us, event | category | flops | bytes accessed | tf_op | source)
XLA Modules:
  0.0 224.9 jit_solution(11564645253851427318)
XLA Ops:
  6.5 0.0 copy-start
  6.6 0.0 copy-start.5
  6.6 0.1 all-gather.2.cloned.1.call-start
  6.6 1.8 pad_maximum_fusion.1
  8.4 0.1 all-gather.2.cloned.1.call-update
  8.5 0.7 fusion.47
  9.2 0.7 maximum_select_fusion
  10.0 91.9 %all_gather.9 = bf16[3072,128]{1,0:T(8,128)(2,1)S(1)} all-gather(bf16[96,128]{1,0:T(8,128)(2,1)S(1)} %maximum_select_fusion), channel_id=1, replica_groups=mesh['grp'=2,'fs'=32,'tp'=8] {'fs'}, dimensions={0}, use_global_device_ids=true | all-gather | bytes 811008 | tf_op jit(solution)/shard_map/all_gather | solution.py:13
  101.8 5.6 %collective-permute-start = (bf16[3072,128]{1,0:T(8,128)(2,1)S(1)}, bf16[3072,128]{1,0:T(8,128)(2,1)S(1)}, u32[]{:S(2)}, u32[]{:S(2)}) collective-permute-start(bf16[3072,128]{1,0:T(8,128)(2,1)S(1)} %all_gather.9), channel_id=1, source_target_pairs={{0,256},{256,0},{1,257},{257,1},{2,258},{258,2},{3,259},{259,3},{4... | collective-permute-start | bytes 2359304 | tf_op jit(solution)/shard_map/ppermute | solution.py:22
  107.5 1.2 convert_reduce_fusion
  108.7 1.3 fusion.23
  110.0 7.2 %collective-permute-done = bf16[3072,128]{1,0:T(8,128)(2,1)S(1)} collective-permute-done((bf16[3072,128]{1,0:T(8,128)(2,1)S(1)}, bf16[3072,128]{1,0:T(8,128)(2,1)S(1)}, u32[]{:S(2)}, u32[]{:S(2)}) %collective-permute-start) | collective-permute-done | bytes 786464 | tf_op jit(solution)/shard_map/ppermute | solution.py:22
  117.2 0.1 broadcast_select_fusion.1
  117.3 0.1 slice.52
  117.4 0.1 slice.53
  117.5 0.0 copy-done.1
  117.5 0.0 copy-done.2
  117.5 0.4 fusion.20
  117.9 0.4 fusion.22
  118.3 0.0 copy-done
  118.3 1.1 fusion.45
  119.4 0.0 copy-done.4
  119.4 0.6 broadcast_in_dim.5
  120.0 15.1 %all-to-all-start = ((f32[8,1,512]{2,1,0:T(1,128)}), f32[8,1,512]{2,1,0:T(1,128)S(1)}, u32[]{:S(2)}, u32[]{:S(2)}) async-start(f32[8,1,512]{2,1,0:T(1,128)} %broadcast_in_dim.5), calls=%async_computation | async-start | bytes 32768 | tf_op jit(solution)/shard_map/all_to_all | solution.py:39
  135.1 0.1 pad_maximum_fusion
  135.2 4.6 %all-to-all-done = f32[8,1,512]{2,1,0:T(1,128)S(1)} async-done(((f32[8,1,512]{2,1,0:T(1,128)}), f32[8,1,512]{2,1,0:T(1,128)S(1)}, u32[]{:S(2)}, u32[]{:S(2)}) %all-to-all-start) | async-done | bytes 16416 | tf_op jit(solution)/shard_map/all_to_all | solution.py:39
  139.8 0.0 copy-done.6
  139.8 0.0 copy-done.5
  139.8 1.2 convolution_convert_fusion
  141.0 4.1 %all-to-all-start.1 = ((bf16[8,16,2048]{2,1,0:T(8,128)(2,1)}), bf16[8,16,2048]{2,1,0:T(8,128)(2,1)S(1)}, u32[]{:S(2)}, u32[]{:S(2)}) async-start(bf16[8,16,2048]{2,1,0:T(8,128)(2,1)} %bitcast.12), calls=%async_computation.1 | async-start | bytes 1048576 | tf_op jit(solution)/shard_map/all_to_all | solution.py:39
  145.2 0.1 dynamic-slice
  145.2 9.4 %all-to-all-done.1 = bf16[8,16,2048]{2,1,0:T(8,128)(2,1)S(1)} async-done(((bf16[8,16,2048]{2,1,0:T(8,128)(2,1)}), bf16[8,16,2048]{2,1,0:T(8,128)(2,1)S(1)}, u32[]{:S(2)}, u32[]{:S(2)}) %all-to-all-start.1) | async-done | bytes 524320 | tf_op jit(solution)/shard_map/all_to_all | solution.py:39
  154.6 0.1 reduce_sum.110
  154.7 0.2 fusion.31
  154.9 0.2 multiply_reduce_fusion.2
  155.1 0.0 copy-done.3
  155.1 0.1 multiply_convert_fusion.1
  155.2 14.0 %all_gather.10 = bf16[128,2048]{1,0:T(8,128)(2,1)S(1)} all-gather(bf16[16,2048]{1,0:T(8,128)(2,1)S(1)} %multiply_convert_fusion.1), channel_id=1, replica_groups=mesh['grp'=2,'fs'=32,'tp'=8] {'tp'}, dimensions={0}, use_global_device_ids=true | all-gather | bytes 589824 | tf_op jit(solution)/shard_map/all_gather | solution.py:121
  169.2 1.2 all-gather.2.cloned.1.call-done
  170.4 6.4 %fusion.4 = bf16[128,2048]{1,0:T(8,128)(2,1)} fusion(bf16[2048,2048]{1,0:T(8,128)(2,1)} %all-gather.2.cloned.1.call-done, bf16[128,2048]{1,0:T(8,128)(2,1)S(1)} %all_gather.10), kind=kOutput, calls=%fused_computation.4 | convolution fusion | flops 1074397184 | bytes 9437184 | tf_op jit(solution)/shard_map/dot_general | solution.py:33
  176.8 22.5 %all-to-all-start.2 = ((bf16[8,16,2048]{2,1,0:T(8,128)(2,1)}), bf16[8,16,2048]{2,1,0:T(8,128)(2,1)S(1)}, u32[]{:S(2)}, u32[]{:S(2)}) async-start(bf16[8,16,2048]{2,1,0:T(8,128)(2,1)} %bitcast.14), calls=%async_computation.2 | async-start | bytes 1048576 | tf_op jit(solution)/shard_map/all_to_all | solution.py:39
  199.2 9.3 %all-to-all-done.2 = bf16[8,16,2048]{2,1,0:T(8,128)(2,1)S(1)} async-done(((bf16[8,16,2048]{2,1,0:T(8,128)(2,1)}), bf16[8,16,2048]{2,1,0:T(8,128)(2,1)S(1)}, u32[]{:S(2)}, u32[]{:S(2)}) %all-to-all-start.2) | async-done | bytes 524320 | tf_op jit(solution)/shard_map/all_to_all | solution.py:39
  208.6 0.1 reduce_sum.113
  208.7 0.1 fusion.32
  208.8 0.2 multiply_reduce_fusion.1
  209.0 0.1 multiply_convert_fusion
  209.1 8.3 %all_to_all.24 = bf16[8,16,256]{2,1,0:T(8,128)(2,1)S(1)} all-to-all(bf16[8,16,256]{2,1,0:T(8,128)(2,1)S(1)} %bitcast.53), channel_id=1, replica_groups=mesh['grp'=2,'fs'=32,'tp'=8] {'tp'}, dimensions={0} | all-to-all | bytes 131072 | tf_op jit(solution)/shard_map/all_to_all | solution.py:39
  217.4 0.6 copy.45
  (19 shorter events, 0.1 us)
Async XLA Ops:
  6.5 111.8 %copy-start = (bf16[31,128]{1,0:T(8,128)(2,1)S(1)}, bf16[31,128]{1,0:T(8,128)(2,1)}, u32[]{:S(2)}) copy-start(bf16[31,128]{1,0:T(8,128)(2,1)} %param.16) | copy-start | bytes 23812
  6.6 111.0 %copy-start.1 = (bf16[1,128,2048]{2,1,0:T(8,128)(2,1)S(1)}, bf16[1,128,2048]{2,1,0:T(8,128)(2,1)}, u32[]{:S(2)}) copy-start(bf16[1,128,2048]{2,1,0:T(8,128)(2,1)} %param.12) | copy-start | bytes 1572868
  6.6 111.0 %copy-start.2 = (f32[2048]{0:T(1024)S(1)}, f32[2048]{0:T(1024)}, u32[]{:S(2)}) copy-start(f32[2048]{0:T(1024)} %param.13) | copy-start | bytes 24580
  6.6 112.9 %copy-start.4 = (f32[256]{0:T(256)S(1)}, f32[256]{0:T(256)}, u32[]{:S(2)}) copy-start(f32[256]{0:T(256)} %param.23) | copy-start | bytes 3076
  6.6 133.3 %copy-start.6 = (f32[128]{0:T(128)S(1)}, f32[128]{0:T(128)}, u32[]{:S(2)}) copy-start(f32[128]{0:T(128)} %param.17) | copy-start | bytes 1540
  6.6 133.3 %copy-start.5 = (f32[128]{0:T(128)S(1)}, f32[128]{0:T(128)}, u32[]{:S(2)}) copy-start(f32[128]{0:T(128)} %param.18) | copy-start | bytes 1540
  6.6 163.8 %all-gather.2.cloned.1.call-start = ((), (), s32[]{:S(2)}) async-start(), calls=%async_computation.4 | async-start | bytes 8650752 | tf_op jit(solution)/shard_map/all_gather | solution.py:13
  101.8 15.4 %collective-permute-start = (bf16[3072,128]{1,0:T(8,128)(2,1)S(1)}, bf16[3072,128]{1,0:T(8,128)(2,1)S(1)}, u32[]{:S(2)}, u32[]{:S(2)}) collective-permute-start(bf16[3072,128]{1,0:T(8,128)(2,1)S(1)} %all_gather.9), channel_id=1, source_target_pairs={{0,256},{256,0},{1,257},{257,1},{2,258},{258,2},{3,259},{259,3},{4... | collective-permute-start | bytes 2359304 | tf_op jit(solution)/shard_map/ppermute | solution.py:22
  108.7 46.4 %copy-start.3 = (f32[2048]{0:T(1024)S(1)}, f32[2048]{0:T(1024)}, u32[]{:S(2)}) copy-start(f32[2048]{0:T(1024)} %param.20) | copy-start | bytes 24580
  120.0 19.7 %all-to-all-start = ((f32[8,1,512]{2,1,0:T(1,128)}), f32[8,1,512]{2,1,0:T(1,128)S(1)}, u32[]{:S(2)}, u32[]{:S(2)}) async-start(f32[8,1,512]{2,1,0:T(1,128)} %broadcast_in_dim.5), calls=%async_computation | async-start | bytes 32768 | tf_op jit(solution)/shard_map/all_to_all | solution.py:39
  141.0 13.6 %all-to-all-start.1 = ((bf16[8,16,2048]{2,1,0:T(8,128)(2,1)}), bf16[8,16,2048]{2,1,0:T(8,128)(2,1)S(1)}, u32[]{:S(2)}, u32[]{:S(2)}) async-start(bf16[8,16,2048]{2,1,0:T(8,128)(2,1)} %bitcast.12), calls=%async_computation.1 | async-start | bytes 1048576 | tf_op jit(solution)/shard_map/all_to_all | solution.py:39
  176.8 31.8 %all-to-all-start.2 = ((bf16[8,16,2048]{2,1,0:T(8,128)(2,1)}), bf16[8,16,2048]{2,1,0:T(8,128)(2,1)S(1)}, u32[]{:S(2)}, u32[]{:S(2)}) async-start(bf16[8,16,2048]{2,1,0:T(8,128)(2,1)} %bitcast.14), calls=%async_computation.2 | async-start | bytes 1048576 | tf_op jit(solution)/shard_map/all_to_all | solution.py:39
Sparse Core Ops, SparseCore 0:
  9.5 160.8 all-gather.1

commit v3 on v2

--- a/solution.py
+++ b/solution.py
@@ -3,24 +3,24 @@
 from jax import lax
 from jax.sharding import PartitionSpec as P
 
+
 KW = 31
 
 norm_epsilon = 1e-05
 residual_scale = 2.0**0.25
+half_scale = 2.0**18
 
 
 def gather_fs(x):
     return lax.all_gather(x, "fs", axis=0, tiled=True)
 
 
-def gather_in_pairs(even_part, odd_part):
-    group_count = lax.axis_size("grp")
-    if group_count % 2:
-        return gather_fs(even_part), gather_fs(odd_part)
-    is_even = lax.axis_index("grp") % 2 == 0
-    mine = gather_fs(jnp.where(is_even, even_part, odd_part))
-    theirs = lax.ppermute(mine, "grp", [(g, g ^ 1) for g in range(group_count)])
-    return jnp.where(is_even, mine, theirs), jnp.where(is_even, theirs, mine)
+def to_half(x):
+    return (x.astype(jnp.float32) * half_scale).astype(jnp.float16)
+
+
+def from_half(x):
+    return (x.astype(jnp.float32) * (1 / half_scale)).astype(jnp.bfloat16)
 
 
 def norm_rows(values, gain_vector):
@@ -68,22 +68,23 @@
     tp_index = lax.axis_index("tp")
     channels = value_weight.shape[1]
 
-    feed = gather_fs(jnp.concatenate([up_weight, down_weight.T], axis=1))
-    hidden_count = up_weight.shape[1]
-    up_whole, down_turned = feed[:, :hidden_count], feed[:, hidden_count:]
+    down_turned = gather_fs(down_weight.T)
 
-    rows = value_weight.shape[0]
-    half = rows // 2
-    out_shard = out_weight.T
-    even_whole, odd_whole = gather_in_pairs(
-        jnp.concatenate([value_weight, out_shard[:half]], axis=0),
-        jnp.concatenate([gate_weight, out_shard[half:]], axis=0),
+    group_count = lax.axis_size("grp")
+    paired = group_count % 2 == 0
+    is_even = lax.axis_index("grp") % 2 == 0
+    hidden_half = up_weight.shape[1] // 2
+    low_up, high_up = up_weight[:, :hidden_half], up_weight[:, hidden_half:]
+    own_up = jnp.where(is_even, low_up, high_up) if paired else up_weight
+    early = gather_fs(
+        to_half(jnp.concatenate([value_weight, gate_weight, out_weight.T, own_up], axis=1))
     )
-    even_whole = even_whole.reshape(-1, rows + half, channels)
-    odd_whole = odd_whole.reshape(-1, rows + half, channels)
-    value_whole = even_whole[:, :rows].reshape(-1, channels)
-    gate_whole = odd_whole[:, :rows].reshape(-1, channels)
-    out_turned = jnp.concatenate([even_whole[:, rows:], odd_whole[:, rows:]], axis=1).reshape(-1, channels)
+    value_whole = from_half(early[:, :channels])
+    gate_whole = from_half(early[:, channels : 2 * channels])
+    out_turned = from_half(early[:, 2 * channels : 3 * channels])
+    up_parts = [early[:, 3 * channels :]]
+    if paired:
+        up_parts.append(lax.ppermute(up_parts[0], "grp", [(g, g ^ 1) for g in range(group_count)]))
 
     normed = norm_rows(
         stream.reshape(token_count, model_width).astype(jnp.float32), in_gain
@@ -120,9 +121,16 @@
     ).astype(jnp.bfloat16)
     settled = lax.all_gather(settled_own, "tp", axis=0, tiled=True)
 
-    hidden = jnp.square(
-        jax.nn.relu(jnp.dot(settled, up_whole, preferred_element_type=jnp.float32))
-    ).astype(jnp.bfloat16)
+    hidden_parts = [
+        jnp.square(
+            jax.nn.relu(jnp.dot(settled, from_half(part), preferred_element_type=jnp.float32))
+        ).astype(jnp.bfloat16)
+        for part in up_parts
+    ]
+    if paired:
+        mine, theirs = hidden_parts
+        hidden_parts = [jnp.where(is_even, mine, theirs), jnp.where(is_even, theirs, mine)]
+    hidden = lax.optimization_barrier(jnp.concatenate(hidden_parts, axis=1))
     fed = summed_tokens(contract(hidden, down_turned))
     result_own = norm_rows(
         residual_scale * settled_own.astype(jnp.float32) + fed.astype(jnp.float32), whole_gain

time: 225 us -> 266 us (1.18)
  blocking collectives: 114 us -> 178 us
  starting transfers between devices: 47.3 us -> 11.7 us
  waiting for transfers between devices: 31.7 us -> 40.4 us
    all_gather x1, blocking collectives: 91.9 us -> 131 us  [gather_fs(): return lax.all_gather(x, 'fs', axis=0, tiled=True)]
    all_to_all x3 -> x2, starting transfers between devices: 41.6 us -> 9.79 us  [swap_blocks(): return lax.all_to_all(x, 'tp', 0, 0, tiled=True)]
    all_to_all x1 -> x2, blocking collectives: 8.25 us -> 32.4 us  [swap_blocks(): return lax.all_to_all(x, 'tp', 0, 0, tiled=True)]
    ppermute x1, waiting for transfers between devices: 7.2 us -> 24.8 us  [shards(): lax.ppermute(up_parts[0], 'grp', [(g, g ^ 1) for g in range(group_count)])]
    all_to_all x3 -> x2, waiting for transfers between devices: 23.3 us -> 14.8 us  [swap_blocks(): return lax.all_to_all(x, 'tp', 0, 0, tiled=True)]
    dot_general x0 -> x2, matrix products: none -> 4.29 us  [shards(): jnp.dot(settled, from_half(part), preferred_element_type=jnp.float32)]
    ppermute x1, starting transfers between devices: 5.63 us -> 1.95 us  [shards(): lax.ppermute(up_parts[0], 'grp', [(g, g ^ 1) for g in range(group_count)])]
  transfers between devices with their start and end apart: 5 -> 4, of which waited for: 5 -> 3; matrix products, arithmetic and copies ran while one was open for 4% -> 6% of each run, Pallas kernels for 0% -> 0%
where the time goes in v3:
time: 266 us; the launch traced here: 265 us
  blocking collectives  178 us (67%)
  waiting for transfers between devices  40.4 us (15%)
  between operations  13.6 us (5%)
  starting transfers between devices  11.7 us (4%)
  matrix products  11.6 us (4%)
  other arithmetic  6.83 us (3%)
  local copies, waits for them, and re-layouts  2.72 us (1%)
    all_gather x1, blocking collectives, gather_fs(): return lax.all_gather(x, 'fs', axis=0, tiled=True)  131 us
    all_to_all x2, blocking collectives, swap_blocks(): return lax.all_to_all(x, 'tp', 0, 0, tiled=True)  32.4 us
    ppermute x1, waiting for transfers between devices, shards(): lax.ppermute(up_parts[0], 'grp', [(g, g ^ 1) for g in range(group_count)])  24.8 us
    all_to_all x2, waiting for transfers between devices, swap_blocks(): return lax.all_to_all(x, 'tp', 0, 0, tiled=True)  14.8 us
    all_gather x1, blocking collectives, shards(): settled = lax.all_gather(settled_own, 'tp', axis=0, tiled=True)  14 us
    all_to_all x2, starting transfers between devices, swap_blocks(): return lax.all_to_all(x, 'tp', 0, 0, tiled=True)  9.79 us
    dot_general x2, matrix products, contract(): lax.dot_general(left, turned, (((1,), (1,)), ((), ())), preferred_element...  5.66 us
  transfers between devices with their start and end apart: 4, of which 3 were waited for; matrix products, arithmetic and copies ran while one was open for 6% of the time, Pallas kernels for 0%

profile of v3, /device:TPU:33, one launch (start us, length us, event | category | flops | bytes accessed | tf_op | source)
XLA Modules:
  0.0 264.8 jit_solution(1668184544484793862)
XLA Ops:
  6.5 0.0 copy-start
  6.6 0.0 all-gather.3.cloned.1.call-start
  6.6 0.7 all-gather.3.cloned.1.call-update
  7.3 0.9 slice_select_fusion
  8.2 0.8 multiply_convert_fusion.22
  9.0 1.2 convert_reduce_fusion
  10.2 1.3 fusion.19
  11.5 1.4 fusion.21
  13.0 0.0 copy-start.3
  13.0 0.0 copy-start.4
  13.0 0.0 copy-start.5
  13.0 131.4 %all-gather.4 = f16[2048,896]{1,0:T(8,128)(2,1)S(1)} all-gather(f16[64,896]{1,0:T(8,128)(2,1)S(1)} %multiply_convert_fusion.22), channel_id=1, replica_groups=mesh['grp'=2,'fs'=32,'tp'=8] {'fs'}, dimensions={0}, use_global_device_ids=true | all-gather | bytes 3784704 | tf_op jit(solution)/shard_map/all_gather | solution.py:15
  144.4 0.0 copy-start.1
  144.4 0.3 fusion.22
  144.7 0.3 fusion.15
  145.1 0.0 copy-done
  145.1 1.1 fusion.46
  146.2 0.1 multiply_reduce_fusion.2
  146.3 0.0 copy-done.3
  146.3 24.2 %all_to_all.24 = f32[8,1,512]{2,1,0:T(1,128)S(1)} all-to-all(f32[8,1,512]{2,1,0:T(1,128)S(1)} %broadcast_in_dim.5), channel_id=1, replica_groups=mesh['grp'=2,'fs'=32,'tp'=8] {'tp'}, dimensions={0} | all-to-all | bytes 32768 | tf_op jit(solution)/shard_map/all_to_all | solution.py:39
  170.5 0.0 copy-done.1
  170.5 0.0 copy-done.4
  170.6 0.0 copy-done.5
  170.6 0.0 copy-start.2
  170.6 1.2 convolution_convert_fusion.1
  171.7 4.1 %all-to-all-start.1 = ((bf16[8,16,2048]{2,1,0:T(8,128)(2,1)}), bf16[8,16,2048]{2,1,0:T(8,128)(2,1)S(1)}, u32[]{:S(2)}, u32[]{:S(2)}) async-start(bf16[8,16,2048]{2,1,0:T(8,128)(2,1)} %bitcast.5), calls=%async_computation.1 | async-start | bytes 1048576 | tf_op jit(solution)/shard_map/all_to_all | solution.py:39
  175.9 2.0 slice.46
  177.9 2.0 collective-permute-start
  179.9 5.4 %all-to-all-done.1 = bf16[8,16,2048]{2,1,0:T(8,128)(2,1)S(1)} async-done(((bf16[8,16,2048]{2,1,0:T(8,128)(2,1)}), bf16[8,16,2048]{2,1,0:T(8,128)(2,1)S(1)}, u32[]{:S(2)}, u32[]{:S(2)}) %all-to-all-start.1) | async-done | bytes 524320 | tf_op jit(solution)/shard_map/all_to_all | solution.py:39
  185.3 0.1 reduce_sum.110
  185.4 0.1 fusion.29
  185.5 0.2 multiply_reduce_fusion.1
  185.7 0.0 copy-done.2
  185.8 0.1 multiply_convert_fusion.24
  185.8 14.0 %all_gather.10 = bf16[128,2048]{1,0:T(8,128)(2,1)S(1)} all-gather(bf16[16,2048]{1,0:T(8,128)(2,1)S(1)} %multiply_convert_fusion.24), channel_id=1, replica_groups=mesh['grp'=2,'fs'=32,'tp'=8] {'tp'}, dimensions={0}, use_global_device_ids=true | all-gather | bytes 589824 | tf_op jit(solution)/shard_map/all_gather | solution.py:122
  199.8 2.1 fusion.8
  202.0 24.8 %collective-permute-done = f16[2048,512]{1,0:T(8,128)(2,1)} collective-permute-done((f16[2048,512]{1,0:T(8,128)(2,1)S(1)}, f16[2048,512]{1,0:T(8,128)(2,1)}, u32[]{:S(2)}, u32[]{:S(2)}) %collective-permute-start) | collective-permute-done | bytes 2097184 | tf_op jit(solution)/shard_map/ppermute | solution.py:87
  226.8 2.2 broadcast_select_fusion.1
  229.0 0.0 all-gather.3.cloned.1.call-done
  229.0 4.5 %convolution_convert_fusion = bf16[128,2048]{1,0:T(8,128)(2,1)} fusion(bf16[128,1024]{1,0:T(8,128)(2,1)S(1)} %pad_maximum_fusion, bf16[2048,1024]{1,0:T(8,128)(2,1)} %all-gather.3.cloned.1.call-done), kind=kOutput, calls=%fused_computation.2 | convolution fusion | flops 537133056 | bytes 4980736 | tf_op jit(solution)/shard_map/dot_general | solution.py:33
  233.5 5.7 %all-to-all-start.2 = ((bf16[8,16,2048]{2,1,0:T(8,128)(2,1)}), bf16[8,16,2048]{2,1,0:T(8,128)(2,1)S(1)}, u32[]{:S(2)}, u32[]{:S(2)}) async-start(bf16[8,16,2048]{2,1,0:T(8,128)(2,1)} %bitcast.7), calls=%async_computation.2 | async-start | bytes 1048576 | tf_op jit(solution)/shard_map/all_to_all | solution.py:39
  239.2 9.3 %all-to-all-done.2 = bf16[8,16,2048]{2,1,0:T(8,128)(2,1)S(1)} async-done(((bf16[8,16,2048]{2,1,0:T(8,128)(2,1)}), bf16[8,16,2048]{2,1,0:T(8,128)(2,1)S(1)}, u32[]{:S(2)}, u32[]{:S(2)}) %all-to-all-start.2) | async-done | bytes 524320 | tf_op jit(solution)/shard_map/all_to_all | solution.py:39
  248.6 0.1 reduce_sum.113
  248.6 0.1 fusion.30
  248.8 0.2 multiply_reduce_fusion
  249.0 0.1 multiply_convert_fusion.23
  249.1 8.3 %all_to_all.25 = bf16[8,16,256]{2,1,0:T(8,128)(2,1)S(1)} all-to-all(bf16[8,16,256]{2,1,0:T(8,128)(2,1)S(1)} %bitcast.44), channel_id=1, replica_groups=mesh['grp'=2,'fs'=32,'tp'=8] {'tp'}, dimensions={0} | all-to-all | bytes 131072 | tf_op jit(solution)/shard_map/all_to_all | solution.py:39
  257.4 0.6 copy.38
  (14 shorter events, 0.1 us)
Async XLA Ops:
  6.5 138.5 %copy-start = (bf16[31,128]{1,0:T(8,128)(2,1)S(1)}, bf16[31,128]{1,0:T(8,128)(2,1)}, u32[]{:S(2)}) copy-start(bf16[31,128]{1,0:T(8,128)(2,1)} %param.16) | copy-start | bytes 23812
  6.6 222.5 %all-gather.3.cloned.1.call-start = ((), (), s32[]{:S(2)}) async-start(), calls=%async_computation.4 | async-start | bytes 4325376 | tf_op jit(solution)/shard_map/all_gather | solution.py:15
  13.0 133.3 %copy-start.3 = (f32[256]{0:T(256)S(1)}, f32[256]{0:T(256)}, u32[]{:S(2)}) copy-start(f32[256]{0:T(256)} %param.23) | copy-start | bytes 3076
  13.0 157.6 %copy-start.4 = (f32[128]{0:T(128)S(1)}, f32[128]{0:T(128)}, u32[]{:S(2)}) copy-start(f32[128]{0:T(128)} %param.18) | copy-start | bytes 1540
  13.0 157.6 %copy-start.5 = (f32[128]{0:T(128)S(1)}, f32[128]{0:T(128)}, u32[]{:S(2)}) copy-start(f32[128]{0:T(128)} %param.17) | copy-start | bytes 1540
  144.4 26.1 %copy-start.1 = (f16[2048,896]{1,0:T(8,128)(2,1)}, f16[2048,896]{1,0:T(8,128)(2,1)S(1)}, u32[]{:S(2)}) copy-start(f16[2048,896]{1,0:T(8,128)(2,1)S(1)} %all-gather.4) | copy-start | bytes 11010052
  170.6 15.2 %copy-start.2 = (f32[2048]{0:T(1024)S(1)}, f32[2048]{0:T(1024)}, u32[]{:S(2)}) copy-start(f32[2048]{0:T(1024)} %param.20) | copy-start | bytes 24580
  171.7 13.6 %all-to-all-start.1 = ((bf16[8,16,2048]{2,1,0:T(8,128)(2,1)}), bf16[8,16,2048]{2,1,0:T(8,128)(2,1)S(1)}, u32[]{:S(2)}, u32[]{:S(2)}) async-start(bf16[8,16,2048]{2,1,0:T(8,128)(2,1)} %bitcast.5), calls=%async_computation.1 | async-start | bytes 1048576 | tf_op jit(solution)/shard_map/all_to_all | solution.py:39
  177.9 48.9 %collective-permute-start = (f16[2048,512]{1,0:T(8,128)(2,1)S(1)}, f16[2048,512]{1,0:T(8,128)(2,1)}, u32[]{:S(2)}, u32[]{:S(2)}) collective-permute-start(f16[2048,512]{1,0:T(8,128)(2,1)S(1)} %slice.46), channel_id=1, source_target_pairs={{0,256},{256,0},{1,257},{257,1},{2,258},{258,2},{3,259},{259,3},{4... | collective-permute-start | bytes 6291464 | tf_op jit(solution)/shard_map/ppermute | solution.py:87
  233.5 15.0 %all-to-all-start.2 = ((bf16[8,16,2048]{2,1,0:T(8,128)(2,1)}), bf16[8,16,2048]{2,1,0:T(8,128)(2,1)S(1)}, u32[]{:S(2)}, u32[]{:S(2)}) async-start(bf16[8,16,2048]{2,1,0:T(8,128)(2,1)} %bitcast.7), calls=%async_computation.2 | async-start | bytes 1048576 | tf_op jit(solution)/shard_map/all_to_all | solution.py:39
Sparse Core Ops, SparseCore 0:
  9.4 153.3 all-gather.2

commit v4 on v2

--- a/solution.py
+++ b/solution.py
@@ -7,20 +7,16 @@
 
 norm_epsilon = 1e-05
 residual_scale = 2.0**0.25
+weight_scale = 2.0**18
+feature_scale = 2.0**7
 
 
-def gather_fs(x):
-    return lax.all_gather(x, "fs", axis=0, tiled=True)
+def to_half(x, scale):
+    return (x.astype(jnp.float32) * scale).astype(jnp.float16)
 
 
-def gather_in_pairs(even_part, odd_part):
-    group_count = lax.axis_size("grp")
-    if group_count % 2:
-        return gather_fs(even_part), gather_fs(odd_part)
-    is_even = lax.axis_index("grp") % 2 == 0
-    mine = gather_fs(jnp.where(is_even, even_part, odd_part))
-    theirs = lax.ppermute(mine, "grp", [(g, g ^ 1) for g in range(group_count)])
-    return jnp.where(is_even, mine, theirs), jnp.where(is_even, theirs, mine)
+def from_half(x, scale):
+    return (x.astype(jnp.float32) * (1 / scale)).astype(jnp.bfloat16)
 
 
 def norm_rows(values, gain_vector):
@@ -39,10 +35,7 @@
     return lax.all_to_all(x, "tp", 0, 0, tiled=True)
 
 
-def summed_tokens(terms):
-    tp_count = lax.axis_size("tp")
-    tokens, width = terms.shape
-    tiles = swap_blocks(terms.astype(jnp.bfloat16).reshape(tp_count, tokens // tp_count, width))
+def summed(tiles):
     return jnp.sum(tiles.astype(jnp.float32), axis=0).astype(jnp.bfloat16)
 
 
@@ -63,27 +56,44 @@
     seq_count, seq_length, model_width = stream.shape
     token_count = seq_count * seq_length
     tp_count = lax.axis_size("tp")
+    group_count = lax.axis_size("grp")
     slice_width = model_width // tp_count
     own_tokens = token_count // tp_count
     tp_index = lax.axis_index("tp")
     channels = value_weight.shape[1]
 
-    feed = gather_fs(jnp.concatenate([up_weight, down_weight.T], axis=1))
-    hidden_count = up_weight.shape[1]
-    up_whole, down_turned = feed[:, :hidden_count], feed[:, hidden_count:]
-
-    rows = value_weight.shape[0]
-    half = rows // 2
-    out_shard = out_weight.T
-    even_whole, odd_whole = gather_in_pairs(
-        jnp.concatenate([value_weight, out_shard[:half]], axis=0),
-        jnp.concatenate([gate_weight, out_shard[half:]], axis=0),
+    sharing = 2 if group_count % 2 == 0 else 1
+    teams = [
+        [g * tp_count + t for g in range(first, first + sharing) for t in range(tp_count)]
+        for first in range(0, group_count, sharing)
+    ]
+    share = up_weight.shape[1] // sharing
+    up_shard, down_shard = up_weight, down_weight.T
+    if sharing == 2:
+        is_even = lax.axis_index("grp") % 2 == 0
+        up_shard = jnp.where(is_even, up_shard[:, :share], up_shard[:, share:])
+        down_shard = jnp.where(is_even, down_shard[:, :share], down_shard[:, share:])
+    whole = lax.all_gather(
+        to_half(
+            jnp.concatenate(
+                [
+                    value_weight,
+                    gate_weight,
+                    out_weight.T,
+                    lax.optimization_barrier(jnp.concatenate([up_shard, down_shard], axis=1)),
+                ],
+                axis=1,
+            ),
+            weight_scale,
+        ),
+        "fs",
+        axis=0,
+        tiled=True,
     )
-    even_whole = even_whole.reshape(-1, rows + half, channels)
-    odd_whole = odd_whole.reshape(-1, rows + half, channels)
-    value_whole = even_whole[:, :rows].reshape(-1, channels)
-    gate_whole = odd_whole[:, :rows].reshape(-1, channels)
-    out_turned = jnp.concatenate([even_whole[:, rows:], odd_whole[:, rows:]], axis=1).reshape(-1, channels)
+    ends = [channels, 2 * channels, 3 * channels, 3 * channels + share]
+    value_whole, gate_whole, out_turned, up_whole, down_turned = (
+        from_half(part, weight_scale) for part in jnp.split(whole, ends, axis=1)
+    )
 
     normed = norm_rows(
         stream.reshape(token_count, model_width).astype(jnp.float32), in_gain
@@ -113,23 +123,43 @@
         + conv_shift
     ).astype(jnp.bfloat16)
 
-    mixed = summed_tokens(contract(activated, out_turned))
+    mixed_terms = contract(activated, out_turned).astype(jnp.bfloat16)
+    mixed = summed(swap_blocks(mixed_terms.reshape(tp_count, own_tokens, model_width)))
     normed_own = lax.dynamic_slice_in_dim(normed, tp_index * own_tokens, own_tokens, 0)
     settled_own = norm_rows(
         residual_scale * normed_own.astype(jnp.float32) + mixed.astype(jnp.float32), norm_gain
     ).astype(jnp.bfloat16)
-    settled = lax.all_gather(settled_own, "tp", axis=0, tiled=True)
+    settled = from_half(
+        lax.all_gather(
+            to_half(settled_own, feature_scale),
+            ("grp", "tp"),
+            axis=0,
+            tiled=True,
+            axis_index_groups=teams,
+        ),
+        feature_scale,
+    )
 
     hidden = jnp.square(
         jax.nn.relu(jnp.dot(settled, up_whole, preferred_element_type=jnp.float32))
     ).astype(jnp.bfloat16)
-    fed = summed_tokens(contract(hidden, down_turned))
+    hidden = lax.optimization_barrier(hidden)
+    fed_terms = contract(hidden, down_turned).astype(jnp.bfloat16)
+    fed = summed(
+        lax.all_to_all(
+            fed_terms.reshape(sharing * tp_count, own_tokens, model_width),
+            ("grp", "tp"),
+            0,
+            0,
+            tiled=True,
+            axis_index_groups=teams,
+        )
+    )
     result_own = norm_rows(
         residual_scale * settled_own.astype(jnp.float32) + fed.astype(jnp.float32), whole_gain
     ).astype(jnp.bfloat16)
     pieces = jnp.moveaxis(result_own.reshape(own_tokens, tp_count, slice_width), 1, 0)
-    result = swap_blocks(pieces)
-    return result.reshape(seq_count, seq_length, slice_width)
+    return swap_blocks(pieces).reshape(seq_count, seq_length, slice_width)
 
 
 def solution(mesh):

time: 225 us -> 234 us (1.040)
  blocking collectives: 114 us -> 184 us
  starting transfers between devices: 47.3 us -> 8.38 us
  between operations: 13.6 us -> 0.2 us
  waiting for transfers between devices: 31.7 us -> 25.1 us
    all_gather x2, blocking collectives: 106 us -> 155 us  [the longest x1 130 us: shards(): lax.all_gather(to_half(jnp.concatenate([value_weight, gate_weight, out_we...]
    all_to_all x3 -> x1, starting transfers between devices: 41.6 us -> 4.12 us  [swap_blocks(): return lax.all_to_all(x, 'tp', 0, 0, tiled=True)]
    all_to_all x1 -> x2, blocking collectives: 8.25 us -> 29 us  [swap_blocks(): return lax.all_to_all(x, 'tp', 0, 0, tiled=True)]
    all_to_all x0 -> x1, waiting for transfers between devices: none -> 15.7 us  [shards(): lax.all_to_all(fed_terms.reshape(sharing * tp_count, own_tokens, model_wi...]
    all_to_all x3 -> x1, waiting for transfers between devices: 23.3 us -> 9.44 us  [swap_blocks(): return lax.all_to_all(x, 'tp', 0, 0, tiled=True)]
    ppermute x1 -> x0, waiting for transfers between devices: 7.2 us -> none  [gather_in_pairs(): theirs = lax.ppermute(mine, 'grp', [(g, g ^ 1) for g in range(group_count)])]
    ppermute x1 -> x0, starting transfers between devices: 5.63 us -> none  [gather_in_pairs(): theirs = lax.ppermute(mine, 'grp', [(g, g ^ 1) for g in range(group_count)])]
    all_to_all x0 -> x1, starting transfers between devices: none -> 4.26 us  [shards(): lax.all_to_all(fed_terms.reshape(sharing * tp_count, own_tokens, model_wi...]
  transfers between devices with their start and end apart: 5 -> 2, of which waited for: 5 -> 2; matrix products, arithmetic and copies ran while one was open for 4% -> 0% of each run, Pallas kernels for 0% -> 0%
where the time goes in v4:
time: 234 us; the launch traced here: 233 us
  blocking collectives  184 us (79%)
  waiting for transfers between devices  25.1 us (11%)
  matrix products  8.56 us (4%)
  starting transfers between devices  8.38 us (4%)
  other arithmetic  6.01 us (3%)
    all_gather x1, blocking collectives, shards(): lax.all_gather(to_half(jnp.concatenate([value_weight, gate_weight, out_we...  130 us
    all_to_all x2, blocking collectives, swap_blocks(): return lax.all_to_all(x, 'tp', 0, 0, tiled=True)  29 us
    all_gather x1, blocking collectives, shards(): lax.all_gather(to_half(settled_own, feature_scale), ('grp', 'tp'), axis=0...  25.2 us
    all_to_all x1, waiting for transfers between devices, shards(): lax.all_to_all(fed_terms.reshape(sharing * tp_count, own_tokens, model_wi...  15.7 us
    all_to_all x1, waiting for transfers between devices, swap_blocks(): return lax.all_to_all(x, 'tp', 0, 0, tiled=True)  9.44 us
  transfers between devices with their start and end apart: 2, of which 2 were waited for; matrix products, arithmetic and copies ran while one was open for 0% of the time, Pallas kernels for 0%

profile of v4, /device:TPU:33, one launch (start us, length us, event | category | flops | bytes accessed | tf_op | source)
XLA Modules:
  0.0 233.0 jit_solution(14539779897741727798)
XLA Ops:
  0.0 0.0 copy-start
  0.0 0.0 copy-start.2
  0.0 0.0 copy-start.3
  0.0 1.3 convert_reduce_fusion
  1.3 1.3 fusion.17
  2.6 1.0 slice_select_fusion
  3.6 0.8 multiply_convert_fusion.18
  4.4 0.0 copy-start.5
  4.4 129.8 %all-gather.2 = f16[2048,1408]{1,0:T(8,128)(2,1)S(1)} all-gather(f16[64,1408]{1,0:T(8,128)(2,1)S(1)} %multiply_convert_fusion.18), channel_id=1, replica_groups=mesh['grp'=2,'fs'=32,'tp'=8] {'fs'}, dimensions={0}, use_global_device_ids=true | all-gather | bytes 5947392 | tf_op jit(solution)/shard_map/all_gather | solution.py:76
  134.3 0.0 copy-done.2
  134.3 0.0 copy-done.3
  134.3 0.0 copy-start.1
  134.3 0.0 copy-start.6
  134.3 0.0 copy-start.7
  134.3 0.0 copy-start.4
  134.3 0.4 fusion.19
  134.7 0.3 fusion.21
  135.0 0.3 fusion.13
  135.3 0.0 copy-done
  135.3 1.1 fusion.47
  136.4 0.1 multiply_reduce_fusion.2
  136.5 0.0 copy-done.5
  136.6 20.8 %all_to_all.24 = f32[8,1,512]{2,1,0:T(1,128)S(1)} all-to-all(f32[8,1,512]{2,1,0:T(1,128)S(1)} %broadcast_in_dim.5), channel_id=1, replica_groups=mesh['grp'=2,'fs'=32,'tp'=8] {'tp'}, dimensions={0} | all-to-all | bytes 32768 | tf_op jit(solution)/shard_map/all_to_all | solution.py:35
  157.3 0.0 copy-done.1
  157.4 0.0 copy-done.6
  157.4 0.0 copy-done.7
  157.4 1.2 convolution_convert_fusion.1
  158.6 4.1 %all-to-all-start.1 = ((bf16[8,16,2048]{2,1,0:T(8,128)(2,1)}), bf16[8,16,2048]{2,1,0:T(8,128)(2,1)S(1)}, u32[]{:S(2)}, u32[]{:S(2)}) async-start(bf16[8,16,2048]{2,1,0:T(8,128)(2,1)} %bitcast.6), calls=%async_computation.1 | async-start | bytes 1048576 | tf_op jit(solution)/shard_map/all_to_all | solution.py:35
  162.7 9.4 %all-to-all-done.1 = bf16[8,16,2048]{2,1,0:T(8,128)(2,1)S(1)} async-done(((bf16[8,16,2048]{2,1,0:T(8,128)(2,1)}), bf16[8,16,2048]{2,1,0:T(8,128)(2,1)S(1)}, u32[]{:S(2)}, u32[]{:S(2)}) %all-to-all-start.1) | async-done | bytes 524320 | tf_op jit(solution)/shard_map/all_to_all | solution.py:35
  172.1 0.1 reduce_sum.110
  172.2 0.1 fusion.30
  172.3 0.2 multiply_reduce_fusion.1
  172.6 0.0 copy-done.4
  172.6 0.1 fusion.29
  172.7 25.2 %all-gather.3 = f16[256,2048]{1,0:T(8,128)(2,1)S(1)} all-gather(f16[16,2048]{1,0:T(8,128)(2,1)S(1)} %get-tuple-element.5), channel_id=1, replica_groups={{0,1,2,3,4,5,6,7,256,257,258,259,260,261,262,263},{8,9,10,11,12,13,14,1..., dimensions={0}, use_global_device_ids=true | all-gather | bytes 1114112 | tf_op jit(solution)/shard_map/all_gather | solution.py:133
  197.9 2.3 %fusion.7 = bf16[256,512]{1,0:T(8,128)(2,1)S(1)} fusion(f16[2048,1408]{1,0:T(8,128)(2,1)} %copy-done.1, f16[256,2048]{1,0:T(8,128)(2,1)S(1)} %all-gather.3), kind=kOutput, calls=%fused_computation.14 | convolution fusion | flops 541982720 | bytes 3407872 | tf_op jit(solution)/shard_map/dot_general | solution.py:144
  200.2 3.3 %convolution_convert_fusion = bf16[256,2048]{1,0:T(8,128)(2,1)} fusion(bf16[256,512]{1,0:T(8,128)(2,1)S(1)} %fusion.7, f16[2048,1408]{1,0:T(8,128)(2,1)} %copy-done.1), kind=kOutput, calls=%fused_computation.2 | convolution fusion | flops 540540928 | bytes 3407872 | tf_op jit(solution)/shard_map/dot_general | solution.py:29
  203.5 4.3 %all-to-all-start.2 = ((bf16[16,16,2048]{2,1,0:T(8,128)(2,1)}), bf16[16,16,2048]{2,1,0:T(8,128)(2,1)S(1)}, u32[]{:S(2)}, u32[]{:S(2)}) async-start(bf16[16,16,2048]{2,1,0:T(8,128)(2,1)} %bitcast.7), calls=%async_computation.2 | async-start | bytes 2097152 | tf_op jit(solution)/shard_map/all_to_all | solution.py:149
  207.8 15.7 %all-to-all-done.2 = bf16[16,16,2048]{2,1,0:T(8,128)(2,1)S(1)} async-done(((bf16[16,16,2048]{2,1,0:T(8,128)(2,1)}), bf16[16,16,2048]{2,1,0:T(8,128)(2,1)S(1)}, u32[]{:S(2)}, u32[]{:S(2)}) %all-to-all-start.2) | async-done | bytes 1048608 | tf_op jit(solution)/shard_map/all_to_all | solution.py:149
  223.5 0.1 reduce_sum.113
  223.6 0.1 fusion.31
  223.8 0.2 multiply_reduce_fusion
  224.0 0.1 multiply_convert_fusion.19
  224.1 8.3 %all_to_all.25 = bf16[8,16,256]{2,1,0:T(8,128)(2,1)S(1)} all-to-all(bf16[8,16,256]{2,1,0:T(8,128)(2,1)S(1)} %bitcast.41), channel_id=1, replica_groups=mesh['grp'=2,'fs'=32,'tp'=8] {'tp'}, dimensions={0} | all-to-all | bytes 131072 | tf_op jit(solution)/shard_map/all_to_all | solution.py:35
  232.3 0.6 copy.38
  (14 shorter events, 0.1 us)
Async XLA Ops:
  0.0 135.3 %copy-start = (bf16[31,128]{1,0:T(8,128)(2,1)S(1)}, bf16[31,128]{1,0:T(8,128)(2,1)}, u32[]{:S(2)}) copy-start(bf16[31,128]{1,0:T(8,128)(2,1)} %param.16) | copy-start | bytes 23812
  0.0 134.3 %copy-start.2 = (bf16[1,128,2048]{2,1,0:T(8,128)(2,1)S(1)}, bf16[1,128,2048]{2,1,0:T(8,128)(2,1)}, u32[]{:S(2)}) copy-start(bf16[1,128,2048]{2,1,0:T(8,128)(2,1)} %param.12) | copy-start | bytes 1572868
  0.0 134.3 %copy-start.3 = (f32[2048]{0:T(1024)S(1)}, f32[2048]{0:T(1024)}, u32[]{:S(2)}) copy-start(f32[2048]{0:T(1024)} %param.13) | copy-start | bytes 24580
  4.4 132.1 %copy-start.5 = (f32[256]{0:T(256)S(1)}, f32[256]{0:T(256)}, u32[]{:S(2)}) copy-start(f32[256]{0:T(256)} %param.23) | copy-start | bytes 3076
  134.3 23.1 %copy-start.1 = (f16[2048,1408]{1,0:T(8,128)(2,1)}, f16[2048,1408]{1,0:T(8,128)(2,1)S(1)}, u32[]{:S(2)}) copy-start(f16[2048,1408]{1,0:T(8,128)(2,1)S(1)} %all-gather.2) | copy-start | bytes 17301508
  134.3 23.1 %copy-start.6 = (f32[128]{0:T(128)S(1)}, f32[128]{0:T(128)}, u32[]{:S(2)}) copy-start(f32[128]{0:T(128)} %param.18) | copy-start | bytes 1540
  134.3 23.1 %copy-start.7 = (f32[128]{0:T(128)S(1)}, f32[128]{0:T(128)}, u32[]{:S(2)}) copy-start(f32[128]{0:T(128)} %param.17) | copy-start | bytes 1540
  134.3 38.3 %copy-start.4 = (f32[2048]{0:T(1024)S(1)}, f32[2048]{0:T(1024)}, u32[]{:S(2)}) copy-start(f32[2048]{0:T(1024)} %param.20) | copy-start | bytes 24580
  158.6 13.6 %all-to-all-start.1 = ((bf16[8,16,2048]{2,1,0:T(8,128)(2,1)}), bf16[8,16,2048]{2,1,0:T(8,128)(2,1)S(1)}, u32[]{:S(2)}, u32[]{:S(2)}) async-start(bf16[8,16,2048]{2,1,0:T(8,128)(2,1)} %bitcast.6), calls=%async_computation.1 | async-start | bytes 1048576 | tf_op jit(solution)/shard_map/all_to_all | solution.py:35
  203.5 19.9 %all-to-all-start.2 = ((bf16[16,16,2048]{2,1,0:T(8,128)(2,1)}), bf16[16,16,2048]{2,1,0:T(8,128)(2,1)S(1)}, u32[]{:S(2)}, u32[]{:S(2)}) async-start(bf16[16,16,2048]{2,1,0:T(8,128)(2,1)} %bitcast.7), calls=%async_computation.2 | async-start | bytes 2097152 | tf_op jit(solution)/shard_map/all_to_all | solution.py:149

commit v5 on v4

--- a/solution.py
+++ b/solution.py
@@ -7,7 +7,6 @@
 
 norm_epsilon = 1e-05
 residual_scale = 2.0**0.25
-weight_scale = 2.0**18
 feature_scale = 2.0**7
 
 
@@ -17,6 +16,14 @@
 
 def from_half(x, scale):
     return (x.astype(jnp.float32) * (1 / scale)).astype(jnp.bfloat16)
+
+
+def gather_fs(x):
+    return lax.all_gather(x, "fs", axis=0, tiled=True)
+
+
+def in_order(is_even, mine, theirs):
+    return jnp.where(is_even, mine, theirs), jnp.where(is_even, theirs, mine)
 
 
 def norm_rows(values, gain_vector):
@@ -63,6 +70,8 @@
     channels = value_weight.shape[1]
 
     sharing = 2 if group_count % 2 == 0 else 1
+    partner = [(g, g ^ 1) for g in range(group_count)]
+    is_even = lax.axis_index("grp") % 2 == 0
     teams = [
         [g * tp_count + t for g in range(first, first + sharing) for t in range(tp_count)]
         for first in range(0, group_count, sharing)
@@ -70,30 +79,27 @@
     share = up_weight.shape[1] // sharing
     up_shard, down_shard = up_weight, down_weight.T
     if sharing == 2:
-        is_even = lax.axis_index("grp") % 2 == 0
         up_shard = jnp.where(is_even, up_shard[:, :share], up_shard[:, share:])
         down_shard = jnp.where(is_even, down_shard[:, :share], down_shard[:, share:])
-    whole = lax.all_gather(
-        to_half(
-            jnp.concatenate(
-                [
-                    value_weight,
-                    gate_weight,
-                    out_weight.T,
-                    lax.optimization_barrier(jnp.concatenate([up_shard, down_shard], axis=1)),
-                ],
-                axis=1,
-            ),
-            weight_scale,
-        ),
-        "fs",
-        axis=0,
-        tiled=True,
-    )
-    ends = [channels, 2 * channels, 3 * channels, 3 * channels + share]
-    value_whole, gate_whole, out_turned, up_whole, down_turned = (
-        from_half(part, weight_scale) for part in jnp.split(whole, ends, axis=1)
-    )
+    feed = gather_fs(jnp.concatenate([up_shard, down_shard], axis=1))
+    up_whole, down_turned = feed[:, :share], feed[:, share:]
+
+    rows = value_weight.shape[0]
+    half = rows // 2
+    out_shard = out_weight.T
+    even_part = jnp.concatenate([value_weight, out_shard[:half]], axis=0)
+    odd_part = jnp.concatenate([gate_weight, out_shard[half:]], axis=0)
+    if sharing == 2:
+        mine = gather_fs(jnp.where(is_even, even_part, odd_part))
+        theirs = lax.ppermute(mine, "grp", partner)
+        even_whole, odd_whole = in_order(is_even, mine, theirs)
+    else:
+        even_whole, odd_whole = gather_fs(even_part), gather_fs(odd_part)
+    even_whole = even_whole.reshape(-1, rows + half, channels)
+    odd_whole = odd_whole.reshape(-1, rows + half, channels)
+    value_whole = even_whole[:, :rows].reshape(-1, channels)
+    gate_whole = odd_whole[:, :rows].reshape(-1, channels)
+    out_turned = jnp.concatenate([even_whole[:, rows:], odd_whole[:, rows:]], axis=1).reshape(-1, channels)
 
     normed = norm_rows(
         stream.reshape(token_count, model_width).astype(jnp.float32), in_gain
@@ -129,16 +135,15 @@
     settled_own = norm_rows(
         residual_scale * normed_own.astype(jnp.float32) + mixed.astype(jnp.float32), norm_gain
     ).astype(jnp.bfloat16)
+    if sharing == 2:
+        their_settled = lax.ppermute(settled_own, "grp", partner)
+        pair_settled = jnp.stack(in_order(is_even, settled_own, their_settled))
+    else:
+        pair_settled = settled_own[None]
     settled = from_half(
-        lax.all_gather(
-            to_half(settled_own, feature_scale),
-            ("grp", "tp"),
-            axis=0,
-            tiled=True,
-            axis_index_groups=teams,
-        ),
+        lax.all_gather(to_half(pair_settled, feature_scale), "tp", axis=1, tiled=True),
         feature_scale,
-    )
+    ).reshape(sharing * token_count, model_width)
 
     hidden = jnp.square(
         jax.nn.relu(jnp.dot(settled, up_whole, preferred_element_type=jnp.float32))

time: 234 us -> 220 us (0.940)
  blocking collectives: 184 us -> 113 us
  starting transfers between devices: 8.38 us -> 37.3 us
  waiting for transfers between devices: 25.1 us -> 41 us
  between operations: 0.2 us -> 13.7 us
  local copies, waits for them, and re-layouts: 0.69 us -> 3.1 us
    all_gather x2, blocking collectives: 155 us -> 104 us  [the longest x1 88.9 us: gather_fs(): return lax.all_gather(x, 'fs', axis=0, tiled=True)]
    all_to_all x2 -> x1, blocking collectives: 29 us -> 8.25 us  [swap_blocks(): return lax.all_to_all(x, 'tp', 0, 0, tiled=True)]
    all_to_all x1 -> x2, starting transfers between devices: 4.12 us -> 20.1 us  [swap_blocks(): return lax.all_to_all(x, 'tp', 0, 0, tiled=True)]
    ppermute x0 -> x2, waiting for transfers between devices: none -> 11.3 us  [the longest x1 9.04 us: shards(): theirs = lax.ppermute(mine, 'grp', partner)]
    ppermute x0 -> x2, starting transfers between devices: none -> 10.5 us  [the longest x1 7.32 us: shards(): theirs = lax.ppermute(mine, 'grp', partner)]
    all_to_all x1 -> x2, waiting for transfers between devices: 9.44 us -> 14 us  [swap_blocks(): return lax.all_to_all(x, 'tp', 0, 0, tiled=True)]
    all_to_all x1, starting transfers between devices: 4.26 us -> 6.75 us  [shards(): lax.all_to_all(fed_terms.reshape(sharing * tp_count, own_tokens, model_wi...]
  transfers between devices with their start and end apart: 2 -> 6, of which waited for: 2 -> 5; matrix products, arithmetic and copies ran while one was open for 0% -> 3% of each run, Pallas kernels for 0% -> 0%
where the time goes in v5:
time: 220 us; the launch traced here: 219 us
  blocking collectives  113 us (51%)
  waiting for transfers between devices  41 us (19%)
  starting transfers between devices  37.3 us (17%)
  between operations  13.7 us (6%)
  matrix products  7.18 us (3%)
  other arithmetic  4.53 us (2%)
  local copies, waits for them, and re-layouts  3.1 us (1%)
    all_gather x1, blocking collectives, gather_fs(): return lax.all_gather(x, 'fs', axis=0, tiled=True)  88.9 us
    all_to_all x2, starting transfers between devices, swap_blocks(): return lax.all_to_all(x, 'tp', 0, 0, tiled=True)  20.1 us
    all_to_all x1, waiting for transfers between devices, shards(): lax.all_to_all(fed_terms.reshape(sharing * tp_count, own_tokens, model_wi...  15.7 us
    all_gather x1, blocking collectives, shards(): lax.all_gather(to_half(pair_settled, feature_scale), 'tp', axis=1, tiled=...  15.5 us
    all_to_all x2, waiting for transfers between devices, swap_blocks(): return lax.all_to_all(x, 'tp', 0, 0, tiled=True)  14 us
    ppermute x1, waiting for transfers between devices, shards(): theirs = lax.ppermute(mine, 'grp', partner)  9.04 us
    all_to_all x1, blocking collectives, swap_blocks(): return lax.all_to_all(x, 'tp', 0, 0, tiled=True)  8.25 us
    ppermute x1, starting transfers between devices, shards(): theirs = lax.ppermute(mine, 'grp', partner)  7.32 us
  transfers between devices with their start and end apart: 6, of which 5 were waited for; matrix products, arithmetic and copies ran while one was open for 3% of the time, Pallas kernels for 0%

profile of v5, /device:TPU:33, one launch (start us, length us, event | category | flops | bytes accessed | tf_op | source)
XLA Modules:
  0.0 219.4 jit_solution(9024882230706043667)
XLA Ops:
  6.6 1.0 slice_select_fusion
  7.6 0.7 pad_maximum_fusion.1
  8.2 0.1 all-gather.3.cloned.1.call-update
  8.3 0.7 fusion.39
  9.0 0.7 maximum_select_fusion
  9.8 88.9 %all_gather.9 = bf16[3072,128]{1,0:T(8,128)(2,1)S(1)} all-gather(bf16[96,128]{1,0:T(8,128)(2,1)S(1)} %maximum_select_fusion), channel_id=1, replica_groups=mesh['grp'=2,'fs'=32,'tp'=8] {'fs'}, dimensions={0}, use_global_device_ids=true | all-gather | bytes 811008 | tf_op jit(solution)/shard_map/all_gather | solution.py:22
  98.7 7.3 %collective-permute-start = (bf16[3072,128]{1,0:T(8,128)(2,1)S(1)}, bf16[3072,128]{1,0:T(8,128)(2,1)S(1)}, u32[]{:S(2)}, u32[]{:S(2)}) collective-permute-start(bf16[3072,128]{1,0:T(8,128)(2,1)S(1)} %all_gather.9), channel_id=1, source_target_pairs={{0,256},{256,0},{1,257},{257,1},{2,258},{258,2},{3,259},{259,3},{4... | collective-permute-start | bytes 2359304 | tf_op jit(solution)/shard_map/ppermute | solution.py:94
  106.0 0.2 convert_reduce_fusion
  106.2 0.3 fusion.17
  106.5 9.0 %collective-permute-done = bf16[3072,128]{1,0:T(8,128)(2,1)S(1)} collective-permute-done((bf16[3072,128]{1,0:T(8,128)(2,1)S(1)}, bf16[3072,128]{1,0:T(8,128)(2,1)S(1)}, u32[]{:S(2)}, u32[]{:S(2)}) %collective-permute-start) | collective-permute-done | bytes 786464 | tf_op jit(solution)/shard_map/ppermute | solution.py:94
  115.5 0.1 broadcast_select_fusion.1
  115.6 0.0 copy-start.2
  115.6 0.1 slice.68
  115.7 0.1 slice.69
  115.8 0.5 copy-done.2
  116.3 0.4 fusion.14
  116.7 0.0 copy-start.5
  116.7 0.0 copy-start.6
  116.8 0.4 fusion.16
  117.1 1.1 fusion.37
  118.2 0.6 broadcast_in_dim.5
  118.9 16.0 %all-to-all-start = ((f32[8,1,512]{2,1,0:T(1,128)}), f32[8,1,512]{2,1,0:T(1,128)S(1)}, u32[]{:S(2)}, u32[]{:S(2)}) async-start(f32[8,1,512]{2,1,0:T(1,128)} %broadcast_in_dim.5), calls=%async_computation | async-start | bytes 32768 | tf_op jit(solution)/shard_map/all_to_all | solution.py:42
  134.8 0.1 pad_maximum_fusion
  134.9 4.6 %all-to-all-done = f32[8,1,512]{2,1,0:T(1,128)S(1)} async-done(((f32[8,1,512]{2,1,0:T(1,128)}), f32[8,1,512]{2,1,0:T(1,128)S(1)}, u32[]{:S(2)}, u32[]{:S(2)}) %all-to-all-start) | async-done | bytes 16416 | tf_op jit(solution)/shard_map/all_to_all | solution.py:42
  139.5 1.2 convolution_convert_fusion.1
  140.7 4.1 %all-to-all-start.1 = ((bf16[8,16,2048]{2,1,0:T(8,128)(2,1)}), bf16[8,16,2048]{2,1,0:T(8,128)(2,1)S(1)}, u32[]{:S(2)}, u32[]{:S(2)}) async-start(bf16[8,16,2048]{2,1,0:T(8,128)(2,1)} %bitcast.12), calls=%async_computation.1 | async-start | bytes 1048576 | tf_op jit(solution)/shard_map/all_to_all | solution.py:42
  144.8 0.1 dynamic-slice
  144.9 9.4 %all-to-all-done.1 = bf16[8,16,2048]{2,1,0:T(8,128)(2,1)S(1)} async-done(((bf16[8,16,2048]{2,1,0:T(8,128)(2,1)}), bf16[8,16,2048]{2,1,0:T(8,128)(2,1)S(1)}, u32[]{:S(2)}, u32[]{:S(2)}) %all-to-all-start.1) | async-done | bytes 524320 | tf_op jit(solution)/shard_map/all_to_all | solution.py:42
  154.3 0.1 reduce_sum.110
  154.3 0.2 fusion.24
  154.6 0.2 multiply_reduce_fusion.2
  154.8 0.1 multiply_convert_fusion.3
  154.9 3.2 %collective-permute-start.1 = (bf16[16,2048]{1,0:T(8,128)(2,1)S(1)}, bf16[16,2048]{1,0:T(8,128)(2,1)S(1)}, u32[]{:S(2)}, u32[]{:S(2)}) collective-permute-start(bf16[16,2048]{1,0:T(8,128)(2,1)S(1)} %multiply_convert_fusion.3), channel_id=1, source_target_pairs={{0,256},{256,0},{1,257},{257,1},{2,258},{258,2},{3,259},{259,3},{4... | collective-permute-start | bytes 196616 | tf_op jit(solution)/shard_map/ppermute | solution.py:139
  158.1 2.2 %collective-permute-done.1 = bf16[16,2048]{1,0:T(8,128)(2,1)S(1)} collective-permute-done((bf16[16,2048]{1,0:T(8,128)(2,1)S(1)}, bf16[16,2048]{1,0:T(8,128)(2,1)S(1)}, u32[]{:S(2)}, u32[]{:S(2)}) %collective-permute-start.1) | collective-permute-done | bytes 65568 | tf_op jit(solution)/shard_map/ppermute | solution.py:139
  160.4 15.5 %all-gather.4 = f16[2,128,2048]{2,1,0:T(8,128)(2,1)S(1)} all-gather(f16[2,16,2048]{2,1,0:T(8,128)(2,1)S(1)} %multiply_convert_fusion.1), channel_id=1, replica_groups=mesh['grp'=2,'fs'=32,'tp'=8] {'tp'}, dimensions={1}, use_global_device_ids=true | all-gather | bytes 1179648 | tf_op jit(solution)/shard_map/all_gather | solution.py:144
  175.8 0.2 multiply_convert_fusion
  176.0 0.0 all-gather.3.cloned.1.call-done
  176.1 2.4 %fusion.9 = bf16[256,512]{1,0:T(8,128)(2,1)S(1)} fusion(bf16[256,2048]{1,0:T(8,128)(2,1)S(1)} %bitcast.56, bf16[2048,1024]{1,0:T(8,128)(2,1)} %all-gather.3.cloned.1.call-done), kind=kOutput, calls=%fused_computation.11 | convolution fusion | flops 537264128 | bytes 3407872 | tf_op jit(solution)/shard_map/dot_general | solution.py:149
  178.5 0.4 copy-done.7
  178.9 1.7 convolution_convert_fusion
  180.6 6.8 %all-to-all-start.2 = ((bf16[16,16,2048]{2,1,0:T(8,128)(2,1)}), bf16[16,16,2048]{2,1,0:T(8,128)(2,1)S(1)}, u32[]{:S(2)}, u32[]{:S(2)}) async-start(bf16[16,16,2048]{2,1,0:T(8,128)(2,1)} %bitcast.17), calls=%async_computation.2 | async-start | bytes 2097152 | tf_op jit(solution)/shard_map/all_to_all | solution.py:154
  187.4 15.7 %all-to-all-done.2 = bf16[16,16,2048]{2,1,0:T(8,128)(2,1)S(1)} async-done(((bf16[16,16,2048]{2,1,0:T(8,128)(2,1)}), bf16[16,16,2048]{2,1,0:T(8,128)(2,1)S(1)}, u32[]{:S(2)}, u32[]{:S(2)}) %all-to-all-start.2) | async-done | bytes 1048608 | tf_op jit(solution)/shard_map/all_to_all | solution.py:154
  203.1 0.1 reduce_sum.113
  203.2 0.1 fusion.25
  203.3 0.2 multiply_reduce_fusion.1
  203.6 0.1 multiply_convert_fusion.2
  203.7 8.3 %all_to_all.24 = bf16[8,16,256]{2,1,0:T(8,128)(2,1)S(1)} all-to-all(bf16[8,16,256]{2,1,0:T(8,128)(2,1)S(1)} %bitcast.60), channel_id=1, replica_groups=mesh['grp'=2,'fs'=32,'tp'=8] {'tp'}, dimensions={0} | all-to-all | bytes 131072 | tf_op jit(solution)/shard_map/all_to_all | solution.py:42
  211.9 0.6 copy.45
  (28 shorter events, 0.2 us)
Async XLA Ops:
  6.5 110.6 %copy-start = (bf16[31,128]{1,0:T(8,128)(2,1)S(1)}, bf16[31,128]{1,0:T(8,128)(2,1)}, u32[]{:S(2)}) copy-start(bf16[31,128]{1,0:T(8,128)(2,1)} %param.16) | copy-start | bytes 23812
  6.6 99.5 %copy-start.1 = (bf16[1,128,2048]{2,1,0:T(8,128)(2,1)S(1)}, bf16[1,128,2048]{2,1,0:T(8,128)(2,1)}, u32[]{:S(2)}) copy-start(bf16[1,128,2048]{2,1,0:T(8,128)(2,1)} %param.12) | copy-start | bytes 1572868
  6.6 169.5 %all-gather.3.cloned.1.call-start = ((), (), s32[]{:S(2)}) async-start(), calls=%async_computation.4 | async-start | bytes 4325376 | tf_op jit(solution)/shard_map/all_gather | solution.py:22
  98.7 16.8 %collective-permute-start = (bf16[3072,128]{1,0:T(8,128)(2,1)S(1)}, bf16[3072,128]{1,0:T(8,128)(2,1)S(1)}, u32[]{:S(2)}, u32[]{:S(2)}) collective-permute-start(bf16[3072,128]{1,0:T(8,128)(2,1)S(1)} %all_gather.9), channel_id=1, source_target_pairs={{0,256},{256,0},{1,257},{257,1},{2,258},{258,2},{3,259},{259,3},{4... | collective-permute-start | bytes 2359304 | tf_op jit(solution)/shard_map/ppermute | solution.py:94
  115.6 0.7 copy-start.2
  116.3 1.9 copy-start.4
  116.7 22.8 %copy-start.5 = (f32[128]{0:T(128)S(1)}, f32[128]{0:T(128)}, u32[]{:S(2)}) copy-start(f32[128]{0:T(128)} %param.18) | copy-start | bytes 1540
  116.7 22.8 %copy-start.6 = (f32[128]{0:T(128)S(1)}, f32[128]{0:T(128)}, u32[]{:S(2)}) copy-start(f32[128]{0:T(128)} %param.17) | copy-start | bytes 1540
  118.9 20.6 %all-to-all-start = ((f32[8,1,512]{2,1,0:T(1,128)}), f32[8,1,512]{2,1,0:T(1,128)S(1)}, u32[]{:S(2)}, u32[]{:S(2)}) async-start(f32[8,1,512]{2,1,0:T(1,128)} %broadcast_in_dim.5), calls=%async_computation | async-start | bytes 32768 | tf_op jit(solution)/shard_map/all_to_all | solution.py:42
  134.8 19.9 %copy-start.3 = (f32[2048]{0:T(1024)S(1)}, f32[2048]{0:T(1024)}, u32[]{:S(2)}) copy-start(f32[2048]{0:T(1024)} %param.20) | copy-start | bytes 24580
  140.7 13.6 %all-to-all-start.1 = ((bf16[8,16,2048]{2,1,0:T(8,128)(2,1)}), bf16[8,16,2048]{2,1,0:T(8,128)(2,1)S(1)}, u32[]{:S(2)}, u32[]{:S(2)}) async-start(bf16[8,16,2048]{2,1,0:T(8,128)(2,1)} %bitcast.12), calls=%async_computation.1 | async-start | bytes 1048576 | tf_op jit(solution)/shard_map/all_to_all | solution.py:42
  154.9 5.4 %collective-permute-start.1 = (bf16[16,2048]{1,0:T(8,128)(2,1)S(1)}, bf16[16,2048]{1,0:T(8,128)(2,1)S(1)}, u32[]{:S(2)}, u32[]{:S(2)}) collective-permute-start(bf16[16,2048]{1,0:T(8,128)(2,1)S(1)} %multiply_convert_fusion.3), channel_id=1, source_target_pairs={{0,256},{256,0},{1,257},{257,1},{2,258},{258,2},{3,259},{259,3},{4... | collective-permute-start | bytes 196616 | tf_op jit(solution)/shard_map/ppermute | solution.py:139
  176.1 2.8 %copy-start.7 = (bf16[2048,1024]{1,0:T(8,128)(2,1)S(1)}, bf16[2048,1024]{1,0:T(8,128)(2,1)}, u32[]{:S(2)}) copy-start(bf16[2048,1024]{1,0:T(8,128)(2,1)} %all-gather.3.cloned.1.call-done) | copy-start | bytes 12582916
  180.6 22.4 %all-to-all-start.2 = ((bf16[16,16,2048]{2,1,0:T(8,128)(2,1)}), bf16[16,16,2048]{2,1,0:T(8,128)(2,1)S(1)}, u32[]{:S(2)}, u32[]{:S(2)}) async-start(bf16[16,16,2048]{2,1,0:T(8,128)(2,1)} %bitcast.17), calls=%async_computation.2 | async-start | bytes 2097152 | tf_op jit(solution)/shard_map/all_to_all | solution.py:154
Sparse Core Ops, SparseCore 0:
  9.4 147.4 all-gather.2

commit v6 on v5

--- a/solution.py
+++ b/solution.py
@@ -119,6 +119,10 @@
     told = jnp.concatenate(
         [jnp.sum(convolved, axis=1), jnp.sum(convolved * convolved, axis=1), out_gain]
     )
+    normed_own = lax.dynamic_slice_in_dim(normed, tp_index * own_tokens, own_tokens, 0)
+    told, out_turned, normed_own, norm_gain = lax.optimization_barrier(
+        (told, out_turned, normed_own, norm_gain)
+    )
     heard = swap_blocks(jnp.broadcast_to(told[None], (tp_count, *told.shape)))
     sums = jnp.sum(heard[:, : 2 * token_count], axis=0).reshape(2, token_count)
     whole_gain = heard[:, 2 * token_count :].reshape(model_width)
@@ -130,8 +134,8 @@
     ).astype(jnp.bfloat16)
 
     mixed_terms = contract(activated, out_turned).astype(jnp.bfloat16)
+    mixed_terms, whole_gain = lax.optimization_barrier((mixed_terms, whole_gain))
     mixed = summed(swap_blocks(mixed_terms.reshape(tp_count, own_tokens, model_width)))
-    normed_own = lax.dynamic_slice_in_dim(normed, tp_index * own_tokens, own_tokens, 0)
     settled_own = norm_rows(
         residual_scale * normed_own.astype(jnp.float32) + mixed.astype(jnp.float32), norm_gain
     ).astype(jnp.bfloat16)

time: 220 us -> 219 us (level)
  blocking collectives: 113 us -> 171 us
  waiting for transfers between devices: 41 us -> 11.2 us
  starting transfers between devices: 37.3 us -> 10.5 us
    all_to_all x1 -> x3, blocking collectives: 8.25 us -> 41.6 us  [swap_blocks(): return lax.all_to_all(x, 'tp', 0, 0, tiled=True)]
    all_to_all x3 -> x0, waiting for transfers between devices: 29.6 us -> none  [the longest x1 15.7 us: shards(): lax.all_to_all(fed_terms.reshape(sharing * tp_count, own_tokens, model_wi...]
    all_to_all x3 -> x0, starting transfers between devices: 26.8 us -> none  [the longest x2 20.1 us: swap_blocks(): return lax.all_to_all(x, 'tp', 0, 0, tiled=True)]
    all_to_all x0 -> x1, blocking collectives: none -> 24.6 us  [shards(): lax.all_to_all(fed_terms.reshape(sharing * tp_count, own_tokens, model_wi...]
  transfers between devices with their start and end apart: 6 -> 3, of which waited for: 5 -> 2; matrix products, arithmetic and copies ran while one was open for 3% -> 3% of each run, Pallas kernels for 0% -> 0%
where the time goes in v6:
time: 219 us; the launch traced here: 218 us
  blocking collectives  171 us (78%)
  between operations  13.7 us (6%)
  waiting for transfers between devices  11.2 us (5%)
  starting transfers between devices  10.5 us (5%)
  matrix products  5.42 us (2%)
  other arithmetic  4.64 us (2%)
    all_gather x1, blocking collectives, gather_fs(): return lax.all_gather(x, 'fs', axis=0, tiled=True)  89.2 us
    all_to_all x3, blocking collectives, swap_blocks(): return lax.all_to_all(x, 'tp', 0, 0, tiled=True)  41.6 us
    all_to_all x1, blocking collectives, shards(): lax.all_to_all(fed_terms.reshape(sharing * tp_count, own_tokens, model_wi...  24.6 us
    all_gather x1, blocking collectives, shards(): lax.all_gather(to_half(pair_settled, feature_scale), 'tp', axis=1, tiled=...  15.3 us
    ppermute x1, waiting for transfers between devices, shards(): theirs = lax.ppermute(mine, 'grp', partner)  9.12 us
    ppermute x1, starting transfers between devices, shards(): theirs = lax.ppermute(mine, 'grp', partner)  6.85 us
  transfers between devices with their start and end apart: 3, of which 2 were waited for; matrix products, arithmetic and copies ran while one was open for 3% of the time, Pallas kernels for 0%

profile of v6, /device:TPU:33, one launch (start us, length us, event | category | flops | bytes accessed | tf_op | source)
XLA Modules:
  0.0 218.2 jit_solution(2994437765599493973)
XLA Ops:
  6.6 1.0 slice_select_fusion
  7.6 0.7 pad_maximum_fusion.1
  8.2 0.1 all-gather.3.cloned.1.call-update
  8.3 0.7 fusion.37
  9.0 0.7 maximum_select_fusion
  9.8 89.2 %all_gather.9 = bf16[3072,128]{1,0:T(8,128)(2,1)S(1)} all-gather(bf16[96,128]{1,0:T(8,128)(2,1)S(1)} %maximum_select_fusion), channel_id=1, replica_groups=mesh['grp'=2,'fs'=32,'tp'=8] {'fs'}, dimensions={0}, use_global_device_ids=true | all-gather | bytes 811008 | tf_op jit(solution)/shard_map/all_gather | solution.py:22
  98.9 6.8 %collective-permute-start = (bf16[3072,128]{1,0:T(8,128)(2,1)S(1)}, bf16[3072,128]{1,0:T(8,128)(2,1)S(1)}, u32[]{:S(2)}, u32[]{:S(2)}) collective-permute-start(bf16[3072,128]{1,0:T(8,128)(2,1)S(1)} %all_gather.9), channel_id=1, source_target_pairs={{0,256},{256,0},{1,257},{257,1},{2,258},{258,2},{3,259},{259,3},{4... | collective-permute-start | bytes 2359304 | tf_op jit(solution)/shard_map/ppermute | solution.py:94
  105.8 0.0 copy-done.1
  105.8 0.2 convert_reduce_fusion
  106.0 0.3 fusion.20
  106.3 0.1 dynamic-slice
  106.3 0.0 copy-done.2
  106.3 0.1 fusion.23
  106.4 9.1 %collective-permute-done = bf16[3072,128]{1,0:T(8,128)(2,1)S(1)} collective-permute-done((bf16[3072,128]{1,0:T(8,128)(2,1)S(1)}, bf16[3072,128]{1,0:T(8,128)(2,1)S(1)}, u32[]{:S(2)}, u32[]{:S(2)}) %collective-permute-start) | collective-permute-done | bytes 786464 | tf_op jit(solution)/shard_map/ppermute | solution.py:94
  115.6 0.1 broadcast_select_fusion.1
  115.7 0.1 slice.69
  115.8 0.1 slice.68
  115.9 0.0 copy-start.4
  115.9 0.4 fusion.14
  116.3 0.0 copy-start.5
  116.3 0.0 copy-start.6
  116.3 0.4 fusion.16
  116.7 1.1 fusion.38
  117.8 0.1 multiply_reduce_fusion.3
  117.9 0.0 copy-start.3
  117.9 0.1 pad_maximum_fusion
  118.0 20.6 %all_to_all.24 = f32[8,1,512]{2,1,0:T(1,128)S(1)} all-to-all(f32[8,1,512]{2,1,0:T(1,128)S(1)} %broadcast_in_dim.5), channel_id=1, replica_groups=mesh['grp'=2,'fs'=32,'tp'=8] {'tp'}, dimensions={0} | all-to-all | bytes 32768 | tf_op jit(solution)/shard_map/all_to_all | solution.py:42
  138.6 0.4 convolution_convert_fusion.1
  139.0 12.5 %all_to_all.25 = bf16[8,16,2048]{2,1,0:T(8,128)(2,1)S(1)} all-to-all(bf16[8,16,2048]{2,1,0:T(8,128)(2,1)S(1)} %bitcast.53), channel_id=1, replica_groups=mesh['grp'=2,'fs'=32,'tp'=8] {'tp'}, dimensions={0} | all-to-all | bytes 1048576 | tf_op jit(solution)/shard_map/all_to_all | solution.py:42
  151.5 0.1 reduce_sum.110
  151.6 0.1 fusion.24
  151.7 0.2 multiply_reduce_fusion.2
  152.0 0.1 multiply_convert_fusion.3
  152.1 3.7 %collective-permute-start.1 = (bf16[16,2048]{1,0:T(8,128)(2,1)S(1)}, bf16[16,2048]{1,0:T(8,128)(2,1)S(1)}, u32[]{:S(2)}, u32[]{:S(2)}) collective-permute-start(bf16[16,2048]{1,0:T(8,128)(2,1)S(1)} %multiply_convert_fusion.3), channel_id=1, source_target_pairs={{0,256},{256,0},{1,257},{257,1},{2,258},{258,2},{3,259},{259,3},{4... | collective-permute-start | bytes 196616 | tf_op jit(solution)/shard_map/ppermute | solution.py:143
  155.8 2.0 collective-permute-done.1
  157.9 15.3 %all-gather.4 = f16[2,128,2048]{2,1,0:T(8,128)(2,1)S(1)} all-gather(f16[2,16,2048]{2,1,0:T(8,128)(2,1)S(1)} %multiply_convert_fusion.1), channel_id=1, replica_groups=mesh['grp'=2,'fs'=32,'tp'=8] {'tp'}, dimensions={1}, use_global_device_ids=true | all-gather | bytes 1179648 | tf_op jit(solution)/shard_map/all_gather | solution.py:148
  173.1 0.2 multiply_convert_fusion
  173.3 0.0 all-gather.3.cloned.1.call-done
  173.4 2.4 %fusion.9 = bf16[256,512]{1,0:T(8,128)(2,1)S(1)} fusion(bf16[256,2048]{1,0:T(8,128)(2,1)S(1)} %bitcast.54, bf16[2048,1024]{1,0:T(8,128)(2,1)} %all-gather.3.cloned.1.call-done), kind=kOutput, calls=%fused_computation.11 | convolution fusion | flops 537264128 | bytes 3407872 | tf_op jit(solution)/shard_map/dot_general | solution.py:153
  175.8 0.4 copy-done.7
  176.2 0.7 convolution_convert_fusion
  176.9 24.6 %all_to_all.26 = bf16[16,16,2048]{2,1,0:T(8,128)(2,1)S(1)} all-to-all(bf16[16,16,2048]{2,1,0:T(8,128)(2,1)S(1)} %bitcast.55), channel_id=1, replica_groups={{0,1,2,3,4,5,6,7,256,257,258,259,260,261,262,263},{8,9,10,11,12,13,14,1..., dimensions={0} | all-to-all | bytes 2097152 | tf_op jit(solution)/shard_map/all_to_all | solution.py:158
  201.6 0.1 reduce_sum.113
  201.7 0.1 fusion.25
  201.8 0.2 multiply_reduce_fusion.1
  202.1 0.1 multiply_convert_fusion.2
  202.2 8.5 %all_to_all.27 = bf16[8,16,256]{2,1,0:T(8,128)(2,1)S(1)} all-to-all(bf16[8,16,256]{2,1,0:T(8,128)(2,1)S(1)} %bitcast.61), channel_id=1, replica_groups=mesh['grp'=2,'fs'=32,'tp'=8] {'tp'}, dimensions={0} | all-to-all | bytes 131072 | tf_op jit(solution)/shard_map/all_to_all | solution.py:42
  210.7 0.6 copy.38
  (27 shorter events, 0.2 us)
Async XLA Ops:
  6.5 110.1 %copy-start = (bf16[31,128]{1,0:T(8,128)(2,1)S(1)}, bf16[31,128]{1,0:T(8,128)(2,1)}, u32[]{:S(2)}) copy-start(bf16[31,128]{1,0:T(8,128)(2,1)} %param.16) | copy-start | bytes 23812
  6.6 99.2 %copy-start.1 = (bf16[1,128,2048]{2,1,0:T(8,128)(2,1)S(1)}, bf16[1,128,2048]{2,1,0:T(8,128)(2,1)}, u32[]{:S(2)}) copy-start(bf16[1,128,2048]{2,1,0:T(8,128)(2,1)} %param.12) | copy-start | bytes 1572868
  6.6 99.8 %copy-start.2 = (f32[2048]{0:T(1024)S(1)}, f32[2048]{0:T(1024)}, u32[]{:S(2)}) copy-start(f32[2048]{0:T(1024)} %param.13) | copy-start | bytes 24580
  6.6 166.8 %all-gather.3.cloned.1.call-start = ((), (), s32[]{:S(2)}) async-start(), calls=%async_computation.4 | async-start | bytes 4325376 | tf_op jit(solution)/shard_map/all_gather | solution.py:22
  98.9 16.6 %collective-permute-start = (bf16[3072,128]{1,0:T(8,128)(2,1)S(1)}, bf16[3072,128]{1,0:T(8,128)(2,1)S(1)}, u32[]{:S(2)}, u32[]{:S(2)}) collective-permute-start(bf16[3072,128]{1,0:T(8,128)(2,1)S(1)} %all_gather.9), channel_id=1, source_target_pairs={{0,256},{256,0},{1,257},{257,1},{2,258},{258,2},{3,259},{259,3},{4... | collective-permute-start | bytes 2359304 | tf_op jit(solution)/shard_map/ppermute | solution.py:94
  115.9 2.0 copy-start.4
  116.3 22.4 %copy-start.5 = (f32[128]{0:T(128)S(1)}, f32[128]{0:T(128)}, u32[]{:S(2)}) copy-start(f32[128]{0:T(128)} %param.18) | copy-start | bytes 1540
  116.3 22.4 %copy-start.6 = (f32[128]{0:T(128)S(1)}, f32[128]{0:T(128)}, u32[]{:S(2)}) copy-start(f32[128]{0:T(128)} %param.17) | copy-start | bytes 1540
  117.9 34.1 %copy-start.3 = (f32[2048]{0:T(1024)S(1)}, f32[2048]{0:T(1024)}, u32[]{:S(2)}) copy-start(f32[2048]{0:T(1024)} %param.20) | copy-start | bytes 24580
  152.1 5.7 %collective-permute-start.1 = (bf16[16,2048]{1,0:T(8,128)(2,1)S(1)}, bf16[16,2048]{1,0:T(8,128)(2,1)S(1)}, u32[]{:S(2)}, u32[]{:S(2)}) collective-permute-start(bf16[16,2048]{1,0:T(8,128)(2,1)S(1)} %multiply_convert_fusion.3), channel_id=1, source_target_pairs={{0,256},{256,0},{1,257},{257,1},{2,258},{258,2},{3,259},{259,3},{4... | collective-permute-start | bytes 196616 | tf_op jit(solution)/shard_map/ppermute | solution.py:143
  173.4 2.8 %copy-start.7 = (bf16[2048,1024]{1,0:T(8,128)(2,1)S(1)}, bf16[2048,1024]{1,0:T(8,128)(2,1)}, u32[]{:S(2)}) copy-start(bf16[2048,1024]{1,0:T(8,128)(2,1)} %all-gather.3.cloned.1.call-done) | copy-start | bytes 12582916
Sparse Core Ops, SparseCore 0:
  9.4 148.0 all-gather.2

commit v7 on v6

--- a/solution.py
+++ b/solution.py
@@ -73,7 +73,7 @@
     partner = [(g, g ^ 1) for g in range(group_count)]
     is_even = lax.axis_index("grp") % 2 == 0
     teams = [
-        [g * tp_count + t for g in range(first, first + sharing) for t in range(tp_count)]
+        [g * tp_count + t for t in range(tp_count) for g in range(first, first + sharing)]
         for first in range(0, group_count, sharing)
     ]
     share = up_weight.shape[1] // sharing
@@ -145,7 +145,7 @@
     else:
         pair_settled = settled_own[None]
     settled = from_half(
-        lax.all_gather(to_half(pair_settled, feature_scale), "tp", axis=1, tiled=True),
+        lax.all_gather(to_half(pair_settled, feature_scale), "tp", axis=0, tiled=True),
         feature_scale,
     ).reshape(sharing * token_count, model_width)
 

time: 219 us -> 218 us (level)
  no operation moved by 1% of the time
where the time goes in v7:
time: 218 us
  blocking collectives  170 us (78%)
  between operations  13.7 us (6%)
  waiting for transfers between devices  11.2 us (5%)
  starting transfers between devices  10.5 us (5%)
  matrix products  5.42 us (2%)
  other arithmetic  4.64 us (2%)
    all_gather x1, blocking collectives, gather_fs(): return lax.all_gather(x, 'fs', axis=0, tiled=True)  89.2 us
    all_to_all x3, blocking collectives, swap_blocks(): return lax.all_to_all(x, 'tp', 0, 0, tiled=True)  41.2 us
    all_to_all x1, blocking collectives, shards(): lax.all_to_all(fed_terms.reshape(sharing * tp_count, own_tokens, model_wi...  24.6 us
    all_gather x1, blocking collectives, shards(): lax.all_gather(to_half(pair_settled, feature_scale), 'tp', axis=0, tiled=...  15.3 us
    ppermute x1, waiting for transfers between devices, shards(): theirs = lax.ppermute(mine, 'grp', partner)  9.12 us
    ppermute x1, starting transfers between devices, shards(): theirs = lax.ppermute(mine, 'grp', partner)  6.85 us
  transfers between devices with their start and end apart: 3, of which 2 were waited for; matrix products, arithmetic and copies ran while one was open for 3% of the time, Pallas kernels for 0%

profile of v7, /device:TPU:33, one launch (start us, length us, event | category | flops | bytes accessed | tf_op | source)
XLA Modules:
  0.0 217.8 jit_solution(2617139166442563405)
XLA Ops:
  6.6 1.0 slice_select_fusion
  7.6 0.7 pad_maximum_fusion.1
  8.2 0.1 all-gather.3.cloned.1.call-update
  8.3 0.7 fusion.37
  9.0 0.7 maximum_select_fusion
  9.8 89.2 %all_gather.9 = bf16[3072,128]{1,0:T(8,128)(2,1)S(1)} all-gather(bf16[96,128]{1,0:T(8,128)(2,1)S(1)} %maximum_select_fusion), channel_id=1, replica_groups=mesh['grp'=2,'fs'=32,'tp'=8] {'fs'}, dimensions={0}, use_global_device_ids=true | all-gather | bytes 811008 | tf_op jit(solution)/shard_map/all_gather | solution.py:22
  98.9 6.8 %collective-permute-start = (bf16[3072,128]{1,0:T(8,128)(2,1)S(1)}, bf16[3072,128]{1,0:T(8,128)(2,1)S(1)}, u32[]{:S(2)}, u32[]{:S(2)}) collective-permute-start(bf16[3072,128]{1,0:T(8,128)(2,1)S(1)} %all_gather.9), channel_id=1, source_target_pairs={{0,256},{256,0},{1,257},{257,1},{2,258},{258,2},{3,259},{259,3},{4... | collective-permute-start | bytes 2359304 | tf_op jit(solution)/shard_map/ppermute | solution.py:94
  105.8 0.0 copy-done.1
  105.8 0.2 convert_reduce_fusion
  106.0 0.3 fusion.20
  106.3 0.1 dynamic-slice
  106.3 0.0 copy-done.2
  106.3 0.1 fusion.23
  106.4 9.1 %collective-permute-done = bf16[3072,128]{1,0:T(8,128)(2,1)S(1)} collective-permute-done((bf16[3072,128]{1,0:T(8,128)(2,1)S(1)}, bf16[3072,128]{1,0:T(8,128)(2,1)S(1)}, u32[]{:S(2)}, u32[]{:S(2)}) %collective-permute-start) | collective-permute-done | bytes 786464 | tf_op jit(solution)/shard_map/ppermute | solution.py:94
  115.6 0.1 broadcast_select_fusion.1
  115.7 0.1 slice.69
  115.8 0.1 slice.68
  115.9 0.0 copy-start.4
  115.9 0.4 fusion.14
  116.3 0.0 copy-start.5
  116.3 0.0 copy-start.6
  116.3 0.4 fusion.16
  116.7 1.1 fusion.38
  117.8 0.1 multiply_reduce_fusion.3
  117.9 0.0 copy-start.3
  117.9 0.1 pad_maximum_fusion
  118.0 20.6 %all_to_all.24 = f32[8,1,512]{2,1,0:T(1,128)S(1)} all-to-all(f32[8,1,512]{2,1,0:T(1,128)S(1)} %broadcast_in_dim.5), channel_id=1, replica_groups=mesh['grp'=2,'fs'=32,'tp'=8] {'tp'}, dimensions={0} | all-to-all | bytes 32768 | tf_op jit(solution)/shard_map/all_to_all | solution.py:42
  138.6 0.4 convolution_convert_fusion.1
  139.0 12.5 %all_to_all.25 = bf16[8,16,2048]{2,1,0:T(8,128)(2,1)S(1)} all-to-all(bf16[8,16,2048]{2,1,0:T(8,128)(2,1)S(1)} %bitcast.53), channel_id=1, replica_groups=mesh['grp'=2,'fs'=32,'tp'=8] {'tp'}, dimensions={0} | all-to-all | bytes 1048576 | tf_op jit(solution)/shard_map/all_to_all | solution.py:42
  151.5 0.1 reduce_sum.110
  151.6 0.1 fusion.24
  151.7 0.2 multiply_reduce_fusion.2
  152.0 0.1 multiply_convert_fusion.3
  152.1 3.7 %collective-permute-start.1 = (bf16[16,2048]{1,0:T(8,128)(2,1)S(1)}, bf16[16,2048]{1,0:T(8,128)(2,1)S(1)}, u32[]{:S(2)}, u32[]{:S(2)}) collective-permute-start(bf16[16,2048]{1,0:T(8,128)(2,1)S(1)} %multiply_convert_fusion.3), channel_id=1, source_target_pairs={{0,256},{256,0},{1,257},{257,1},{2,258},{258,2},{3,259},{259,3},{4... | collective-permute-start | bytes 196616 | tf_op jit(solution)/shard_map/ppermute | solution.py:143
  155.8 2.0 collective-permute-done.1
  157.9 15.3 %all-gather.4 = f16[16,16,2048]{2,1,0:T(8,128)(2,1)S(1)} all-gather(f16[2,16,2048]{2,1,0:T(8,128)(2,1)S(1)} %multiply_convert_fusion.1), channel_id=1, replica_groups=mesh['grp'=2,'fs'=32,'tp'=8] {'tp'}, dimensions={0}, use_global_device_ids=true | all-gather | bytes 1179648 | tf_op jit(solution)/shard_map/all_gather | solution.py:148
  173.1 0.2 multiply_convert_fusion
  173.3 0.0 all-gather.3.cloned.1.call-done
  173.4 2.4 %fusion.9 = bf16[256,512]{1,0:T(8,128)(2,1)S(1)} fusion(bf16[256,2048]{1,0:T(8,128)(2,1)S(1)} %bitcast.54, bf16[2048,1024]{1,0:T(8,128)(2,1)} %all-gather.3.cloned.1.call-done), kind=kOutput, calls=%fused_computation.11 | convolution fusion | flops 537264128 | bytes 3407872 | tf_op jit(solution)/shard_map/dot_general | solution.py:153
  175.8 0.4 copy-done.7
  176.2 0.7 convolution_convert_fusion
  176.9 24.6 %all_to_all.26 = bf16[16,16,2048]{2,1,0:T(8,128)(2,1)S(1)} all-to-all(bf16[16,16,2048]{2,1,0:T(8,128)(2,1)S(1)} %bitcast.55), channel_id=1, replica_groups={{0,256,1,257,2,258,3,259,4,260,5,261,6,262,7,263},{8,264,9,265,10,266,1..., dimensions={0} | all-to-all | bytes 2097152 | tf_op jit(solution)/shard_map/all_to_all | solution.py:158
  201.5 0.1 reduce_sum.113
  201.7 0.1 fusion.25
  201.8 0.2 multiply_reduce_fusion.1
  202.0 0.1 multiply_convert_fusion.2
  202.1 8.1 %all_to_all.27 = bf16[8,16,256]{2,1,0:T(8,128)(2,1)S(1)} all-to-all(bf16[8,16,256]{2,1,0:T(8,128)(2,1)S(1)} %bitcast.61), channel_id=1, replica_groups=mesh['grp'=2,'fs'=32,'tp'=8] {'tp'}, dimensions={0} | all-to-all | bytes 131072 | tf_op jit(solution)/shard_map/all_to_all | solution.py:42
  210.3 0.6 copy.44
  (27 shorter events, 0.2 us)
Async XLA Ops:
  6.5 110.1 %copy-start = (bf16[31,128]{1,0:T(8,128)(2,1)S(1)}, bf16[31,128]{1,0:T(8,128)(2,1)}, u32[]{:S(2)}) copy-start(bf16[31,128]{1,0:T(8,128)(2,1)} %param.16) | copy-start | bytes 23812
  6.6 99.2 %copy-start.1 = (bf16[1,128,2048]{2,1,0:T(8,128)(2,1)S(1)}, bf16[1,128,2048]{2,1,0:T(8,128)(2,1)}, u32[]{:S(2)}) copy-start(bf16[1,128,2048]{2,1,0:T(8,128)(2,1)} %param.12) | copy-start | bytes 1572868
  6.6 99.8 %copy-start.2 = (f32[2048]{0:T(1024)S(1)}, f32[2048]{0:T(1024)}, u32[]{:S(2)}) copy-start(f32[2048]{0:T(1024)} %param.13) | copy-start | bytes 24580
  6.6 166.8 %all-gather.3.cloned.1.call-start = ((), (), s32[]{:S(2)}) async-start(), calls=%async_computation.4 | async-start | bytes 4325376 | tf_op jit(solution)/shard_map/all_gather | solution.py:22
  98.9 16.6 %collective-permute-start = (bf16[3072,128]{1,0:T(8,128)(2,1)S(1)}, bf16[3072,128]{1,0:T(8,128)(2,1)S(1)}, u32[]{:S(2)}, u32[]{:S(2)}) collective-permute-start(bf16[3072,128]{1,0:T(8,128)(2,1)S(1)} %all_gather.9), channel_id=1, source_target_pairs={{0,256},{256,0},{1,257},{257,1},{2,258},{258,2},{3,259},{259,3},{4... | collective-permute-start | bytes 2359304 | tf_op jit(solution)/shard_map/ppermute | solution.py:94
  115.9 2.0 copy-start.4
  116.3 22.4 %copy-start.5 = (f32[128]{0:T(128)S(1)}, f32[128]{0:T(128)}, u32[]{:S(2)}) copy-start(f32[128]{0:T(128)} %param.18) | copy-start | bytes 1540
  116.3 22.4 %copy-start.6 = (f32[128]{0:T(128)S(1)}, f32[128]{0:T(128)}, u32[]{:S(2)}) copy-start(f32[128]{0:T(128)} %param.17) | copy-start | bytes 1540
  117.9 34.1 %copy-start.3 = (f32[2048]{0:T(1024)S(1)}, f32[2048]{0:T(1024)}, u32[]{:S(2)}) copy-start(f32[2048]{0:T(1024)} %param.20) | copy-start | bytes 24580
  152.1 5.7 %collective-permute-start.1 = (bf16[16,2048]{1,0:T(8,128)(2,1)S(1)}, bf16[16,2048]{1,0:T(8,128)(2,1)S(1)}, u32[]{:S(2)}, u32[]{:S(2)}) collective-permute-start(bf16[16,2048]{1,0:T(8,128)(2,1)S(1)} %multiply_convert_fusion.3), channel_id=1, source_target_pairs={{0,256},{256,0},{1,257},{257,1},{2,258},{258,2},{3,259},{259,3},{4... | collective-permute-start | bytes 196616 | tf_op jit(solution)/shard_map/ppermute | solution.py:143
  173.4 2.8 %copy-start.7 = (bf16[2048,1024]{1,0:T(8,128)(2,1)S(1)}, bf16[2048,1024]{1,0:T(8,128)(2,1)}, u32[]{:S(2)}) copy-start(bf16[2048,1024]{1,0:T(8,128)(2,1)} %all-gather.3.cloned.1.call-done) | copy-start | bytes 12582916
Sparse Core Ops, SparseCore 0:
  9.4 148.0 all-gather.2

commit v8 on v7

--- a/solution.py
+++ b/solution.py
@@ -20,6 +20,16 @@
 
 def gather_fs(x):
     return lax.all_gather(x, "fs", axis=0, tiled=True)
+
+
+def gather_in_strides(x):
+    count = lax.axis_size("fs")
+    if count % 2:
+        return gather_fs(x)
+    pairs = [[i, i + 1] for i in range(0, count, 2)]
+    strides = [list(range(first, count, 2)) for first in range(2)]
+    both = lax.all_gather(x, "fs", axis=0, tiled=True, axis_index_groups=pairs)
+    return lax.all_gather(both, "fs", axis=0, tiled=True, axis_index_groups=strides)
 
 
 def in_order(is_even, mine, theirs):
@@ -90,7 +100,7 @@
     even_part = jnp.concatenate([value_weight, out_shard[:half]], axis=0)
     odd_part = jnp.concatenate([gate_weight, out_shard[half:]], axis=0)
     if sharing == 2:
-        mine = gather_fs(jnp.where(is_even, even_part, odd_part))
+        mine = gather_in_strides(jnp.where(is_even, even_part, odd_part))
         theirs = lax.ppermute(mine, "grp", partner)
         even_whole, odd_whole = in_order(is_even, mine, theirs)
     else:

time: 218 us -> 220 us (level)
  blocking collectives: 170 us -> 175 us
  starting transfers between devices: 10.5 us -> 7.12 us
    all_to_all x1, blocking collectives: 24.6 us -> 38 us  [shards(): lax.all_to_all(fed_terms.reshape(sharing * tp_count, own_tokens, model_wi...]
    all_gather x1 -> x2, blocking collectives: 89.2 us -> 81.3 us  [the longest x1 76 us: gather_in_strides(): lax.all_gather(both, 'fs', axis=0, tiled=True, axis_index_groups=strides)]
    ppermute x1, starting transfers between devices: 6.85 us -> 3.64 us  [shards(): theirs = lax.ppermute(mine, 'grp', partner)]
where the time goes in v8:
time: 220 us; the launch traced here: 219 us
  blocking collectives  175 us (80%)
  between operations  13.7 us (6%)
  waiting for transfers between devices  11.6 us (5%)
  starting transfers between devices  7.12 us (3%)
  matrix products  5.39 us (2%)
  other arithmetic  4.64 us (2%)
    all_gather x1, blocking collectives, gather_in_strides(): lax.all_gather(both, 'fs', axis=0, tiled=True, axis_index_groups=strides)  76 us
    all_to_all x3, blocking collectives, swap_blocks(): return lax.all_to_all(x, 'tp', 0, 0, tiled=True)  39.8 us
    all_to_all x1, blocking collectives, shards(): lax.all_to_all(fed_terms.reshape(sharing * tp_count, own_tokens, model_wi...  38 us
    all_gather x1, blocking collectives, shards(): lax.all_gather(to_half(pair_settled, feature_scale), 'tp', axis=0, tiled=...  15.5 us
    ppermute x1, waiting for transfers between devices, shards(): theirs = lax.ppermute(mine, 'grp', partner)  9.51 us
    all_gather x1, blocking collectives, gather_in_strides(): both = lax.all_gather(x, 'fs', axis=0, tiled=True, axis_index_groups=pairs)  5.27 us
  transfers between devices with their start and end apart: 3, of which 2 were waited for; matrix products, arithmetic and copies ran while one was open for 3% of the time, Pallas kernels for 0%

profile of v8, /device:TPU:33, one launch (start us, length us, event | category | flops | bytes accessed | tf_op | source)
XLA Modules:
  0.0 219.0 jit_solution(9094577985772962188)
XLA Ops:
  6.6 0.0 all-gather.3.cloned.1.call-start
  6.6 1.0 slice_select_fusion
  7.6 0.7 pad_maximum_fusion.1
  8.2 0.1 all-gather.3.cloned.1.call-update
  8.3 0.7 fusion.37
  9.0 0.7 maximum_select_fusion
  9.8 5.3 %all_gather.12 = bf16[192,128]{1,0:T(8,128)(2,1)S(1)} all-gather(bf16[96,128]{1,0:T(8,128)(2,1)S(1)} %maximum_select_fusion), channel_id=1, replica_groups={{0,8},{16,24},{32,40},{48,56},{64,72},{80,88},{96,104},{112,120},{128,1..., dimensions={0}, use_global_device_ids=true | all-gather | bytes 73728 | tf_op jit(solution)/shard_map/all_gather | solution.py:31
  15.0 76.0 %all_gather.13 = bf16[3072,128]{1,0:T(8,128)(2,1)S(1)} all-gather(bf16[192,128]{1,0:T(8,128)(2,1)S(1)} %all_gather.12), channel_id=1, replica_groups={{0,16,32,48,64,80,96,112,128,144,160,176,192,208,224,240},{8,24,40,56,7..., dimensions={0}, use_global_device_ids=true | all-gather | bytes 835584 | tf_op jit(solution)/shard_map/all_gather | solution.py:32
  91.0 3.6 %collective-permute-start = (bf16[3072,128]{1,0:T(8,128)(2,1)S(1)}, bf16[3072,128]{1,0:T(8,128)(2,1)S(1)}, u32[]{:S(2)}, u32[]{:S(2)}) collective-permute-start(bf16[3072,128]{1,0:T(8,128)(2,1)S(1)} %all_gather.13), channel_id=1, source_target_pairs={{0,256},{256,0},{1,257},{257,1},{2,258},{258,2},{3,259},{259,3},{4... | collective-permute-start | bytes 2359304 | tf_op jit(solution)/shard_map/ppermute | solution.py:104
  94.7 0.2 convert_reduce_fusion
  94.9 0.3 fusion.20
  95.2 0.1 dynamic-slice
  95.3 0.1 fusion.23
  95.3 9.5 %collective-permute-done = bf16[3072,128]{1,0:T(8,128)(2,1)S(1)} collective-permute-done((bf16[3072,128]{1,0:T(8,128)(2,1)S(1)}, bf16[3072,128]{1,0:T(8,128)(2,1)S(1)}, u32[]{:S(2)}, u32[]{:S(2)}) %collective-permute-start) | collective-permute-done | bytes 786464 | tf_op jit(solution)/shard_map/ppermute | solution.py:104
  104.9 0.1 broadcast_select_fusion.1
  105.0 0.1 slice.69
  105.1 0.1 slice.68
  105.2 0.0 copy-start.4
  105.2 0.4 fusion.14
  105.6 0.0 copy-start.5
  105.6 0.0 copy-start.6
  105.6 0.4 fusion.16
  106.0 1.1 fusion.38
  107.1 0.1 multiply_reduce_fusion.3
  107.2 0.0 copy-start.3
  107.2 0.1 pad_maximum_fusion
  107.3 19.2 %all_to_all.24 = f32[8,1,512]{2,1,0:T(1,128)S(1)} all-to-all(f32[8,1,512]{2,1,0:T(1,128)S(1)} %broadcast_in_dim.5), channel_id=1, replica_groups=mesh['grp'=2,'fs'=32,'tp'=8] {'tp'}, dimensions={0} | all-to-all | bytes 32768 | tf_op jit(solution)/shard_map/all_to_all | solution.py:52
  126.6 0.4 convolution_convert_fusion.1
  127.0 12.5 %all_to_all.25 = bf16[8,16,2048]{2,1,0:T(8,128)(2,1)S(1)} all-to-all(bf16[8,16,2048]{2,1,0:T(8,128)(2,1)S(1)} %bitcast.53), channel_id=1, replica_groups=mesh['grp'=2,'fs'=32,'tp'=8] {'tp'}, dimensions={0} | all-to-all | bytes 1048576 | tf_op jit(solution)/shard_map/all_to_all | solution.py:52
  139.4 0.1 reduce_sum.110
  139.5 0.1 fusion.24
  139.6 0.2 multiply_reduce_fusion.2
  139.9 0.1 multiply_convert_fusion.3
  139.9 3.5 %collective-permute-start.1 = (bf16[16,2048]{1,0:T(8,128)(2,1)S(1)}, bf16[16,2048]{1,0:T(8,128)(2,1)S(1)}, u32[]{:S(2)}, u32[]{:S(2)}) collective-permute-start(bf16[16,2048]{1,0:T(8,128)(2,1)S(1)} %multiply_convert_fusion.3), channel_id=1, source_target_pairs={{0,256},{256,0},{1,257},{257,1},{2,258},{258,2},{3,259},{259,3},{4... | collective-permute-start | bytes 196616 | tf_op jit(solution)/shard_map/ppermute | solution.py:153
  143.4 2.0 collective-permute-done.1
  145.5 15.5 %all-gather.4 = f16[16,16,2048]{2,1,0:T(8,128)(2,1)S(1)} all-gather(f16[2,16,2048]{2,1,0:T(8,128)(2,1)S(1)} %multiply_convert_fusion.1), channel_id=1, replica_groups=mesh['grp'=2,'fs'=32,'tp'=8] {'tp'}, dimensions={0}, use_global_device_ids=true | all-gather | bytes 1179648 | tf_op jit(solution)/shard_map/all_gather | solution.py:158
  161.0 0.2 multiply_convert_fusion
  161.2 0.0 all-gather.3.cloned.1.call-done
  161.2 2.4 %fusion.9 = bf16[256,512]{1,0:T(8,128)(2,1)S(1)} fusion(bf16[256,2048]{1,0:T(8,128)(2,1)S(1)} %bitcast.54, bf16[2048,1024]{1,0:T(8,128)(2,1)} %all-gather.3.cloned.1.call-done), kind=kOutput, calls=%fused_computation.11 | convolution fusion | flops 537264128 | bytes 3407872 | tf_op jit(solution)/shard_map/dot_general | solution.py:163
  163.7 0.4 copy-done.7
  164.1 0.7 convolution_convert_fusion
  164.8 38.0 %all_to_all.26 = bf16[16,16,2048]{2,1,0:T(8,128)(2,1)S(1)} all-to-all(bf16[16,16,2048]{2,1,0:T(8,128)(2,1)S(1)} %bitcast.55), channel_id=1, replica_groups={{0,256,1,257,2,258,3,259,4,260,5,261,6,262,7,263},{8,264,9,265,10,266,1..., dimensions={0} | all-to-all | bytes 2097152 | tf_op jit(solution)/shard_map/all_to_all | solution.py:168
  202.8 0.1 reduce_sum.113
  202.9 0.1 fusion.25
  203.1 0.2 multiply_reduce_fusion.1
  203.3 0.1 multiply_convert_fusion.2
  203.4 8.1 %all_to_all.27 = bf16[8,16,256]{2,1,0:T(8,128)(2,1)S(1)} all-to-all(bf16[8,16,256]{2,1,0:T(8,128)(2,1)S(1)} %bitcast.61), channel_id=1, replica_groups=mesh['grp'=2,'fs'=32,'tp'=8] {'tp'}, dimensions={0} | all-to-all | bytes 131072 | tf_op jit(solution)/shard_map/all_to_all | solution.py:52
  211.5 0.6 copy.44
  (28 shorter events, 0.2 us)
Async XLA Ops:
  6.5 99.4 %copy-start = (bf16[31,128]{1,0:T(8,128)(2,1)S(1)}, bf16[31,128]{1,0:T(8,128)(2,1)}, u32[]{:S(2)}) copy-start(bf16[31,128]{1,0:T(8,128)(2,1)} %param.16) | copy-start | bytes 23812
  6.6 88.1 %copy-start.1 = (bf16[1,128,2048]{2,1,0:T(8,128)(2,1)S(1)}, bf16[1,128,2048]{2,1,0:T(8,128)(2,1)}, u32[]{:S(2)}) copy-start(bf16[1,128,2048]{2,1,0:T(8,128)(2,1)} %param.12) | copy-start | bytes 1572868
  6.6 88.7 %copy-start.2 = (f32[2048]{0:T(1024)S(1)}, f32[2048]{0:T(1024)}, u32[]{:S(2)}) copy-start(f32[2048]{0:T(1024)} %param.13) | copy-start | bytes 24580
  6.6 154.7 %all-gather.3.cloned.1.call-start = ((), (), s32[]{:S(2)}) async-start(), calls=%async_computation.4 | async-start | bytes 4325376 | tf_op jit(solution)/shard_map/all_gather | solution.py:22
  91.0 13.8 %collective-permute-start = (bf16[3072,128]{1,0:T(8,128)(2,1)S(1)}, bf16[3072,128]{1,0:T(8,128)(2,1)S(1)}, u32[]{:S(2)}, u32[]{:S(2)}) collective-permute-start(bf16[3072,128]{1,0:T(8,128)(2,1)S(1)} %all_gather.13), channel_id=1, source_target_pairs={{0,256},{256,0},{1,257},{257,1},{2,258},{258,2},{3,259},{259,3},{4... | collective-permute-start | bytes 2359304 | tf_op jit(solution)/shard_map/ppermute | solution.py:104
  105.2 2.0 copy-start.4
  105.6 21.0 %copy-start.5 = (f32[128]{0:T(128)S(1)}, f32[128]{0:T(128)}, u32[]{:S(2)}) copy-start(f32[128]{0:T(128)} %param.18) | copy-start | bytes 1540
  105.6 21.0 %copy-start.6 = (f32[128]{0:T(128)S(1)}, f32[128]{0:T(128)}, u32[]{:S(2)}) copy-start(f32[128]{0:T(128)} %param.17) | copy-start | bytes 1540
  107.2 32.7 %copy-start.3 = (f32[2048]{0:T(1024)S(1)}, f32[2048]{0:T(1024)}, u32[]{:S(2)}) copy-start(f32[2048]{0:T(1024)} %param.20) | copy-start | bytes 24580
  139.9 5.5 %collective-permute-start.1 = (bf16[16,2048]{1,0:T(8,128)(2,1)S(1)}, bf16[16,2048]{1,0:T(8,128)(2,1)S(1)}, u32[]{:S(2)}, u32[]{:S(2)}) collective-permute-start(bf16[16,2048]{1,0:T(8,128)(2,1)S(1)} %multiply_convert_fusion.3), channel_id=1, source_target_pairs={{0,256},{256,0},{1,257},{257,1},{2,258},{258,2},{3,259},{259,3},{4... | collective-permute-start | bytes 196616 | tf_op jit(solution)/shard_map/ppermute | solution.py:153
  161.2 2.8 %copy-start.7 = (bf16[2048,1024]{1,0:T(8,128)(2,1)S(1)}, bf16[2048,1024]{1,0:T(8,128)(2,1)}, u32[]{:S(2)}) copy-start(bf16[2048,1024]{1,0:T(8,128)(2,1)} %all-gather.3.cloned.1.call-done) | copy-start | bytes 12582916
Sparse Core Ops, SparseCore 0:
  9.4 149.9 all-gather.2
